TPU v7x, 256 devices: a whole 4x4x8 slice. The times are simulated.
256 devices in a mesh: fs: 32 (over z, y), tp: 8 (over x, core).
Axes of the slice: x: 4, y: 4, z: 8, core: 2. Of those that a mesh axis runs over, the one named last changes fastest.
Arguments:
- normed_input: bfloat16 [16384, 2048], P('fs', 'tp'), may hold values from -6 to 6
- cotangent: bfloat16 [16384, 2048], P('fs', 'tp'), may hold values from -6 to 6
- up_weight: bfloat16 [2048, 8192], P('fs', 'tp'), may hold values from -0.125 to 0.125
- down_weight: bfloat16 [8192, 2048], P('tp', 'fs'), may hold values from -0.0625 to 0.0625
Outputs:
- input_grad: bfloat16 [16384, 2048], P('fs', 'tp')
- up_grad: float32 [2048, 8192], P('fs', 'tp')
- down_grad: float32 [8192, 2048], P('tp', 'fs')
All inputs are finite; a program needn't handle non-finite values.
Results may differ from a plain program's by a relative error of at most 0.018.
Values may be sent and summed in bfloat16 or wider, within the bound.
A program may use at most 64 MiB of HBM per device.

v0:
```python
import jax
import jax.numpy as jnp
from jax import lax
from jax.sharding import Mesh
from jax.sharding import PartitionSpec as P

FS = ("fs_0", "fs_1")


def in_one_piece(arrays, axis, dim, along):
    ends, at = ([], 0)
    for a in arrays[:-1]:
        at += a.shape[along]
        ends.append(at)
    both = jnp.concatenate(arrays, axis=along)
    return tuple(jnp.split(lax.all_gather(both, axis, axis=dim, tiled=True), ends, axis=along))


def whole_of(value, axes, dim):
    for axis in reversed(axes):
        value = lax.all_gather(value, axis, axis=dim, tiled=True)
    return value


def in_blocks(value, dim, count):
    shape = value.shape
    pieces = value.reshape(*shape[:dim], count, shape[dim] // count, *shape[dim + 1 :])
    return jnp.moveaxis(pieces, dim, 0)


def sent_and_summed(value, axis, dim):
    pieces = in_blocks(value, dim, lax.axis_size(axis))
    arrived = lax.all_to_all(pieces, axis, split_axis=0, concat_axis=0, tiled=True)
    return arrived.astype(jnp.float32).sum(axis=0)


def sum_by_axis(terms, axes):
    subtotal = terms.astype(jnp.bfloat16)
    for axis in axes:
        subtotal = lax.psum_scatter(subtotal, axis, scatter_dimension=0, tiled=True)
    return subtotal.astype(jnp.float32)


def sum_by_axis_2(value, axes, dim):
    for axis in axes:
        value = lax.psum_scatter(value, axis, scatter_dimension=dim, tiled=True)
    return value


def right_product(left, right):
    return lax.dot_general(
        left, right, (((1,), (1,)), ((), ())), preferred_element_type=jnp.float32
    )


def left_product(left, right):
    return lax.dot_general(
        left, right, (((0,), (0,)), ((), ())), preferred_element_type=jnp.float32
    )


def per_device(normed_input, cotangent, up_weight, down_weight):
    whole_input, whole_cot = in_one_piece((normed_input, cotangent), "tp", 1, 0)
    rows = whole_input.shape[0]
    tokens = rows * lax.axis_size(FS)
    scale = lax.rsqrt(jnp.asarray(tokens, jnp.float32))
    block = whole_cot
    act_grad = right_product(block, whole_of(down_weight, FS, 1))
    whole_up = whole_of(up_weight, FS, 0)
    pre = jnp.dot(whole_input, whole_up, preferred_element_type=jnp.float32)
    rectified = jax.nn.relu(pre)
    act = (rectified * rectified).astype(jnp.bfloat16)
    pre_grad = (2.0 * rectified * act_grad).astype(jnp.bfloat16)
    partial_value = right_product(pre_grad, whole_up)
    input_grad = sent_and_summed(partial_value.astype(jnp.bfloat16), "tp", 1).astype(jnp.bfloat16)
    block = whole_input
    up_grad = sum_by_axis(left_product(block, pre_grad) * scale, FS)
    down_term = left_product(act, whole_cot) * scale
    down_grad = sum_by_axis_2(down_term.astype(jnp.bfloat16), FS, 1).astype(jnp.float32)
    return (input_grad, up_grad, down_grad)


def solution(mesh):
    split = Mesh(mesh.devices.reshape(8, 4, mesh.shape["tp"]), ("fs_0", "fs_1", "tp"))
    in_specs = (P(FS, "tp"), P(FS, "tp"), P(FS, "tp"), P("tp", FS))
    out_specs = (P(FS, "tp"), P(FS, "tp"), P("tp", FS))
    return jax.shard_map(
        per_device, mesh=split, in_specs=in_specs, out_specs=out_specs, check_vma=False
    )
```

profile of v0, /device:TPU:1, one launch (start us, length us, event | category | flops | bytes accessed | tf_op | source)
XLA Modules:
  0.0 335.0 jit_solution(13063535587174434972)
XLA Ops:
  7.2 0.0 all-gather.4.cloned.1.call-start
  7.2 1.9 pad_maximum_fusion
  9.1 0.0 all-gather.4.cloned.1.call-update
  9.1 0.0 all-gather.6.cloned.1.call-start
  9.2 13.3 %all_gather.16 = bf16[256,1024]{1,0:T(8,128)(2,1)} all-gather(bf16[64,1024]{1,0:T(8,128)(2,1)} %param.6), channel_id=1, replica_groups=mesh['fs_0'=8,'fs_1'=4,'tp'=8] {'fs_1'}, dimensions={0}, use_global_device_ids=true | all-gather | bytes 655360 | tf_op jit(solution)/shard_map/all_gather | solution.py:21
  22.5 0.0 all-gather.6.cloned.1.call-update
  22.5 0.0 all-gather.8.cloned.1.call-start
  22.5 11.4 %all_gather.18 = bf16[1024,256]{0,1:T(8,128)(2,1)} all-gather(bf16[1024,64]{0,1:T(8,128)(2,1)} %param.7), channel_id=1, replica_groups=mesh['fs_0'=8,'fs_1'=4,'tp'=8] {'fs_1'}, dimensions={1}, use_global_device_ids=true | all-gather | bytes 655360 | tf_op jit(solution)/shard_map/all_gather | solution.py:21
  33.9 0.0 all-gather.8.cloned.1.call-update
  34.0 0.0 reduce-scatter.11.cloned.1.call-start
  34.0 18.1 %all-gather.4.cloned.1.call-done = bf16[1024,2048]{1,0:T(8,128)(2,1)} async-done(((bf16[1024,256]{1,0:T(8,128)(2,1)}), bf16[1024,2048]{1,0:T(8,128)(2,1)}) %all-gather.4.cloned.1.call-update) | async-done | bytes 4194320 | tf_op jit(solution)/shard_map/all_gather | solution.py:16
  52.1 57.0 %all-gather.6.cloned.1.call-done = bf16[2048,1024]{1,0:T(8,128)(2,1)} async-done(((bf16[256,1024]{1,0:T(8,128)(2,1)}), bf16[2048,1024]{1,0:T(8,128)(2,1)}) %all-gather.6.cloned.1.call-update) | async-done | bytes 4194320 | tf_op jit(solution)/shard_map/all_gather | solution.py:21
  109.0 0.0 copy-start
  109.0 5.3 %fusion.4 = f32[512,1024]{1,0:T(8,128)S(1)} fusion(bf16[2048,1024]{1,0:T(8,128)(2,1)} %all-gather.6.cloned.1.call-done, bf16[1024,2048]{1,0:T(8,128)(2,1)} %all-gather.4.cloned.1.call-done), kind=kOutput, calls=%fused_computation.10 | convolution fusion | flops 2147483648 | bytes 8388608 | tf_op jit(solution)/shard_map/dot_general | solution.py:70
  114.3 0.0 copy-done
  114.4 4.4 %multiply_convert_fusion = bf16[1024,2048]{1,0:T(8,128)(2,1)} fusion(bf16[1024,2048]{1,0:T(8,128)(2,1)S(1)} %copy-done, f32[512,1024]{1,0:T(8,128)S(1)} %fusion.4), kind=kOutput, calls=%fused_computation | convolution fusion | flops 2153250816 | bytes 8388608 | tf_op jit(solution)/shard_map/dot_general | solution.py:57
  118.7 0.0 reduce-scatter.11.cloned.1.call-update
  118.8 0.0 reduce-scatter.7.cloned.1.call-start
  118.8 45.4 %all-gather.8.cloned.1.call-done = bf16[1024,2048]{0,1:T(8,128)(2,1)} async-done(((bf16[1024,256]{0,1:T(8,128)(2,1)}), bf16[1024,2048]{0,1:T(8,128)(2,1)}) %all-gather.8.cloned.1.call-update) | async-done | bytes 4194320 | tf_op jit(solution)/shard_map/all_gather | solution.py:21
  164.2 0.0 copy-start.1
  164.2 5.3 %multiply_convert_fusion.3 = bf16[512,1024]{1,0:T(8,128)(2,1)S(1)} fusion(f32[512,1024]{1,0:T(8,128)S(1)} %fusion.4, bf16[1024,2048]{0,1:T(8,128)(2,1)} %all-gather.8.cloned.1.call-done, bf16[1024,2048]{1,0:T(8,128)(2,1)} %all-gather.4.cloned.1.call-done), kind=kOutput, calls=%fused_computation.5 | convolution fusion | flops 2149580800 | bytes 9437184 | tf_op jit(solution)/shard_map/dot_general | solution.py:51
  169.5 0.0 copy-done.1
  169.5 4.4 %multiply_convert_fusion.1 = bf16[2048,1024]{1,0:T(8,128)(2,1)} fusion(bf16[512,1024]{1,0:T(8,128)(2,1)S(1)} %multiply_convert_fusion.3, bf16[1024,2048]{1,0:T(8,128)(2,1)S(1)} %copy-done.1), kind=kOutput, calls=%fused_computation.1 | convolution fusion | flops 2151677952 | bytes 7340032 | tf_op jit(solution)/shard_map/dot_general | solution.py:57
  173.9 0.0 reduce-scatter.7.cloned.1.call-update
  173.9 0.0 reduce-scatter.13.cloned.1.call-start
  174.0 46.7 %reduce-scatter.11.cloned.1.call-done = bf16[1024,256]{1,0:T(8,128)(2,1)} async-done(((bf16[1024,2048]{1,0:T(8,128)(2,1)}), bf16[1024,256]{1,0:T(8,128)(2,1)}) %reduce-scatter.11.cloned.1.call-update) | async-done | bytes 524304 | tf_op jit(solution)/shard_map/reduce_scatter | solution.py:46
  220.7 2.1 copy.10
  222.8 0.0 reduce-scatter.13.cloned.1.call-update
  222.8 4.6 %convolution_convert_fusion = bf16[512,2048]{1,0:T(8,128)(2,1)S(1)} fusion(bf16[512,1024]{1,0:T(8,128)(2,1)S(1)} %multiply_convert_fusion.3, bf16[2048,1024]{1,0:T(8,128)(2,1)} %all-gather.6.cloned.1.call-done), kind=kOutput, calls=%fused_computation.2 | convolution fusion | flops 2148532224 | bytes 7340032 | tf_op jit(solution)/shard_map/dot_general | solution.py:51
  227.3 1.5 copy.14
  228.8 5.0 %all-to-all-start = ((bf16[8,512,256]{2,1,0:T(8,128)(2,1)}), bf16[8,512,256]{2,1,0:T(8,128)(2,1)S(1)}, u32[]{:S(2)}, u32[]{:S(2)}) async-start(bf16[8,512,256]{2,1,0:T(8,128)(2,1)} %bitcast.14), calls=%async_computation | async-start | bytes 4194304 | tf_op jit(solution)/shard_map/all_to_all | solution.py:33
  233.8 0.0 reduce-scatter.9.cloned.1.call-start
  233.8 43.3 %reduce-scatter.7.cloned.1.call-done = bf16[256,1024]{1,0:T(8,128)(2,1)} async-done(((bf16[2048,1024]{1,0:T(8,128)(2,1)}), bf16[256,1024]{1,0:T(8,128)(2,1)}) %reduce-scatter.7.cloned.1.call-update) | async-done | bytes 524304 | tf_op jit(solution)/shard_map/reduce_scatter | solution.py:40
  277.1 0.0 reduce-scatter.9.cloned.1.call-update
  277.1 0.0 all-to-all-done
  277.1 1.0 reduce_sum.12
  278.2 21.9 %reduce-scatter.13.cloned.1.call-done = bf16[64,1024]{1,0:T(8,128)(2,1)} async-done(((bf16[256,1024]{1,0:T(8,128)(2,1)}), bf16[64,1024]{1,0:T(8,128)(2,1)}) %reduce-scatter.13.cloned.1.call-update) | async-done | bytes 131088
  300.1 1.1 copy.11
  301.1 0.8 copy.9
  302.0 24.6 %reduce-scatter.9.cloned.1.call-done = bf16[64,1024]{1,0:T(8,128)(2,1)} async-done(((bf16[256,1024]{1,0:T(8,128)(2,1)}), bf16[64,1024]{1,0:T(8,128)(2,1)}) %reduce-scatter.9.cloned.1.call-update) | async-done | bytes 131088 | tf_op jit(solution)/shard_map/reduce_scatter | solution.py:40
  326.6 1.6 convert_element_type.26
Async XLA Ops:
  7.2 44.9 %all-gather.4.cloned.1.call-start = ((), (), s32[]{:S(2)}) async-start(), calls=%async_computation.5 | async-start | bytes 4718592 | tf_op jit(solution)/shard_map/all_gather | solution.py:16
  9.1 99.9 %all-gather.6.cloned.1.call-start = ((), (), s32[]{:S(2)}) async-start(), calls=%async_computation.6 | async-start | bytes 4718592 | tf_op jit(solution)/shard_map/all_gather | solution.py:21
  22.5 141.7 %all-gather.8.cloned.1.call-start = ((), (), s32[]{:S(2)}) async-start(), calls=%async_computation.7 | async-start | bytes 4718592 | tf_op jit(solution)/shard_map/all_gather | solution.py:21
  34.0 186.7 %reduce-scatter.11.cloned.1.call-start = ((), (), s32[]{:S(2)}) async-start(), calls=%async_computation.10 | async-start | bytes 4718592 | tf_op jit(solution)/shard_map/reduce_scatter | solution.py:46
  109.0 5.3 %copy-start = (bf16[1024,2048]{1,0:T(8,128)(2,1)S(1)}, bf16[1024,2048]{1,0:T(8,128)(2,1)}, u32[]{:S(2)}) copy-start(bf16[1024,2048]{1,0:T(8,128)(2,1)} %all-gather.4.cloned.1.call-done) | copy-start | bytes 12582916
  118.8 158.3 %reduce-scatter.7.cloned.1.call-start = ((), (), s32[]{:S(2)}) async-start(), calls=%async_computation.8 | async-start | bytes 4718592 | tf_op jit(solution)/shard_map/reduce_scatter | solution.py:40
  164.2 5.3 %copy-start.1 = (bf16[1024,2048]{1,0:T(8,128)(2,1)S(1)}, bf16[1024,2048]{1,0:T(8,128)(2,1)}, u32[]{:S(2)}) copy-start(bf16[1024,2048]{1,0:T(8,128)(2,1)} %all-gather.4.cloned.1.call-done) | copy-start | bytes 12582916
  173.9 126.1 %reduce-scatter.13.cloned.1.call-start = ((), (), s32[]{:S(2)}) async-start(), calls=%async_computation.11 | async-start | bytes 655360
  228.8 48.3 %all-to-all-start = ((bf16[8,512,256]{2,1,0:T(8,128)(2,1)}), bf16[8,512,256]{2,1,0:T(8,128)(2,1)S(1)}, u32[]{:S(2)}, u32[]{:S(2)}) async-start(bf16[8,512,256]{2,1,0:T(8,128)(2,1)} %bitcast.14), calls=%async_computation | async-start | bytes 4194304 | tf_op jit(solution)/shard_map/all_to_all | solution.py:33
  233.8 92.8 %reduce-scatter.9.cloned.1.call-start = ((), (), s32[]{:S(2)}) async-start(), calls=%async_computation.9 | async-start | bytes 655360 | tf_op jit(solution)/shard_map/reduce_scatter | solution.py:40
Sparse Core Ops, SparseCore 0:
  9.8 42.2 all-gather.3
  53.9 55.1 all-gather.5
  110.8 53.3 all-gather.7
  166.6 54.0 reduce-scatter.10
  223.1 53.9 reduce-scatter.6
  279.5 20.5 reduce-scatter.12
  302.6 23.9 reduce-scatter.8
where the time goes:
time: 337 us; the launch traced here: 335 us
  waiting for transfers between devices  257 us (76%)
  blocking collectives  24.7 us (7%)
  matrix products  23.9 us (7%)
  between operations  14.2 us (4%)
  local copies, waits for them, and re-layouts  5.46 us (2%)
  starting transfers between devices  5.23 us (2%)
  other arithmetic  4.57 us (1%)
    all_gather x2, waiting for transfers between devices, whole_of(): value = lax.all_gather(value, axis, axis=dim, tiled=True)  102 us
    reduce_scatter x2, waiting for transfers between devices, sum_by_axis(): subtotal = lax.psum_scatter(subtotal, axis, scatter_dimension=0, tiled=True)  67.9 us
    reduce_scatter x1, waiting for transfers between devices, sum_by_axis_2(): value = lax.psum_scatter(value, axis, scatter_dimension=dim, tiled=True)  46.7 us
    all_gather x2, blocking collectives, whole_of(): value = lax.all_gather(value, axis, axis=dim, tiled=True)  24.7 us
    unnamed x8, waiting for transfers between devices  22 us
    all_gather x1, waiting for transfers between devices, in_one_piece(): lax.all_gather(both, axis, axis=dim, tiled=True)  18.1 us
    dot_general x2, matrix products, right_product(): lax.dot_general(left, right, (((1,), (1,)), ((), ())), preferred_element_...  9.85 us
    dot_general x2, matrix products, left_product(): lax.dot_general(left, right, (((0,), (0,)), ((), ())), preferred_element_...  8.75 us
  transfers between devices with their start and end apart: 8, of which 7 were waited for; matrix products, arithmetic and copies ran while one was open for 9% of the time, Pallas kernels for 0%

commit v1 on v0

v1 whole, which is shorter than its diff:
```python
import jax
import jax.numpy as jnp
from jax import lax
from jax.experimental import pallas as pl
from jax.experimental.pallas import tpu as pltpu
from jax.sharding import PartitionSpec as P

NX, NY, NZ = 4, 4, 8
D = 2048
TB = 256
FX = 512
HB = 256
DZ = 256
RY = 64
HALF = TB // 2
QUART = TB // 4
COPIES = 152
MESH = pl.DeviceIdType.MESH
BF16, F32 = jnp.bfloat16, jnp.float32


def nn(a, b):
    return lax.dot_general(a, b, (((1,), (0,)), ((), ())), preferred_element_type=F32)


def nt(a, b):
    return lax.dot_general(a, b, (((1,), (1,)), ((), ())), preferred_element_type=F32)


def kernel(
    x_in, c_in, up_in, dn_in, ig_out, ug_out, dg_out,
    xb, cb, w, xs, cs, uv, pg, tr, gt, gs, pb, rz, sz, fs_s, fs_r, g,
    ra, rb, sb, q1, rc, rd, sd, re, rf, sf, q2, rg, rh, sh, fp, rp,
    lsem, ssem, rsem,
):
    fs, tp = lax.axis_index("fs"), lax.axis_index("tp")
    z, y = lax.div(fs, NY), lax.rem(fs, NY)
    x, c = lax.div(tp, 2), lax.rem(tp, 2)
    o = 1 - c
    step = lambda a, k, n: lax.rem(a + (k % n), n)
    xr, xl, x2 = step(x, 1, NX), step(x, -1, NX), step(x, 2, NX)
    yr, yl, y2 = step(y, 1, NY), step(y, -1, NY), step(y, 2, NY)
    at = lambda ax, ay, az, ac: (az * NY + ay, ax * 2 + ac)
    XR, XL = at(xr, y, z, c), at(xl, y, z, c)
    YR, YL, Y2 = at(x, yr, z, c), at(x, yl, z, c), at(x, y2, z, c)
    ZR, ZL = at(x, y, step(z, 1, NZ), c), at(x, y, step(z, -1, NZ), c)
    PC = at(x, y, z, o)

    ids = iter(range(COPIES))
    sent = []

    def send(src, dst, where):
        i = next(ids)
        copy = pltpu.make_async_remote_copy(
            src_ref=src, dst_ref=dst, send_sem=ssem.at[i], recv_sem=rsem.at[i],
            device_id=where, device_id_type=MESH,
        )
        copy.start()
        sent.append(copy)
        return copy

    def cols(k, n):
        return pl.ds(pl.multiple_of(k * n, n), n)

    mine = lambda k: pl.ds(pl.multiple_of(x * FX + k * 256, 256), 256)
    loads = []
    for i, (src, dst) in enumerate((
        (x_in.at[cols(o, TB), :], xs),
        (c_in.at[cols(o, TB), :], cs),
        (x_in.at[cols(c, TB), :], xb.at[y, :, mine(c)]),
        (c_in.at[cols(c, TB), :], cb.at[y, :, mine(c)]),
        (up_in, uv.at[0]),
        (dn_in, uv.at[1]),
        (up_in.at[:, cols(y, HB)], w.at[0, c, pl.ds(pl.multiple_of(z * DZ + y * RY, RY), RY), :]),
        (dn_in.at[:, cols(y, HB)], w.at[1, c, pl.ds(pl.multiple_of(z * DZ + y * RY, RY), RY), :]),
    )):
        copy = pltpu.make_async_copy(src, dst, lsem.at[i])
        copy.start()
        loads.append(copy)

    barrier = pltpu.get_barrier_semaphore()
    peers = (XR, XL, YR, YL, Y2, ZR, ZL, PC)
    for peer in peers:
        pl.semaphore_signal(barrier, inc=1, device_id=peer, device_id_type=MESH)
    pl.semaphore_wait(barrier, len(peers))

    loads[1].wait()
    cop = send(cs, cb.at[y, :, mine(c)], PC)
    loads[0].wait()
    xop = send(xs, xb.at[y, :, mine(c)], PC)
    loads[4].wait()
    loads[5].wait()
    wrow = pl.ds(pl.multiple_of(z * DZ + y * RY, RY), RY)
    wops = []
    for ay, where in ((y2, Y2), (yr, YR), (yl, YL)):
        for u in range(2):
            wops.append(send(uv.at[u, :, cols(ay, HB)], w.at[u, c, wrow, :], where))

    def blk(buf, ay, ax, half=None):
        rows = slice(None) if half is None else pl.ds(half * HALF, HALF)
        return buf.at[ay, rows, cols(ax, FX)]

    def both(buf, ay, ax, ways, half=None):
        ref = blk(buf, ay, ax, half)
        return [send(ref, ref, way) for way in ways]

    XX, YY = (XR, XL), (YR, YL)
    loads[2].wait()
    loads[3].wait()
    cop.wait_recv()
    c_y = {"me": both(cb, y, x, YY)}
    xop.wait_recv()
    x_x = both(xb, y, x, XX)
    x_y = {"me": both(xb, y, x, YY)}
    c_x = {"me": both(cb, y, x, XX)}

    loads[6].wait()
    loads[7].wait()
    for op in wops:
        op.wait_recv()

    def zblk(u, az):
        return w.at[u, c, cols(az, DZ), :]

    wz = [[], []]
    wpc = []
    order = ([(0, 0), (1, 0), (0, 1), (1, 1), (0, 2), (1, 2), (0, 3)],
             [(1, 0), (0, 0), (1, 1), (0, 1), (1, 2), (0, 2), (1, 3)])

    def wsend(way, i):
        u, k = order[way][i]
        ref = zblk(u, step(z, -k if way == 0 else k, NZ))
        wz[way].append(send(ref, ref, (ZR, ZL)[way]))

    for i in range(2):
        for way in range(2):
            wsend(way, i)
    for u in range(2):
        wpc.append(send(zblk(u, z), zblk(u, z), PC))

    def warrive(i):
        for way in range(2):
            wz[way][i].wait_recv()
            u, k = order[way][i]
            if i + 2 < 7:
                wsend(way, i + 2)
            ref = zblk(u, step(z, -(k + 1) if way == 0 else k + 1, NZ))
            wpc.append(send(ref, ref, PC))

    def got(ops):
        for op in ops:
            op.wait_recv()

    def pass_x(ay, ops):
        ops[0].wait_recv()
        a = blk(cb, ay, xl, 0)
        first = send(a, a, XR)
        ops[1].wait_recv()
        b = blk(cb, ay, xr, 1)
        return [first, send(b, b, XL)]

    def pass_y(ax, ops):
        ops[0].wait_recv()
        a = blk(xb, yl, ax, 0)
        first = send(a, a, YR)
        ops[1].wait_recv()
        b = blk(xb, yr, ax, 1)
        return [first, send(b, b, YL)]

    x_x[0].wait_recv()
    a = blk(xb, y, xl, 0)
    fx = [send(a, a, XR)]
    x_x[1].wait_recv()
    b = blk(xb, y, xr, 1)
    fx.append(send(b, b, XL))
    c_y["me"][0].wait_recv()
    a = blk(cb, yl, x, 0)
    fc = [send(a, a, YR)]
    c_y["me"][1].wait_recv()
    b = blk(cb, yr, x, 1)
    fc.append(send(b, b, YL))
    warrive(0)
    warrive(1)
    fcx = {"me": pass_x(y, c_x["me"])}
    x_y["l"] = both(xb, y, xl, YY)
    c_x["l"] = both(cb, yl, x, XX)
    x_y["r"] = both(xb, y, xr, YY)
    c_x["r"] = both(cb, yr, x, XX)
    warrive(2)
    got(fx)
    x_y["2"] = both(xb, y, x2, YY)
    got(fc)
    warrive(3)
    warrive(4)
    fxy = {"me": pass_y(x, x_y["me"])}
    warrive(5)
    fcx["l"] = pass_x(yl, c_x["l"])
    fxy["l"] = pass_y(xl, x_y["l"])
    warrive(6)
    got(fcx["me"])
    got(wpc)

    def forward(ay):
        for h in range(2):
            pre = nn(xb[ay], w[0, h])
            act_grad = nn(cb[ay], w[1, h])
            rect = jnp.maximum(pre, 0.0)
            grad = 2.0 * rect * act_grad
            pg[:, h * HB:(h + 1) * HB] = grad.astype(BF16)
            tr[0, h * HB:(h + 1) * HB, :] = grad.T.astype(BF16)
            tr[1, h * HB:(h + 1) * HB, :] = (rect * rect).T.astype(BF16)

    def partial(ay):
        @pl.loop(0, NZ)
        def _(k):
            rows = cols(k, DZ)
            total = nt(pg[:, :HB], w[0, 0, rows, :]) + nt(pg[:, HB:], w[0, 1, rows, :])
            g[ay, :, rows] = total.astype(BF16)

    def weights(ay, first):
        for u, buf in ((0, xb), (1, cb)):
            @pl.loop(0, NZ)
            def _(k):
                term = nn(tr[u], buf[ay, :, cols(k, DZ)])
                gt[u, k] = term if first else gt[u, k] + term

    forward(y)
    weights(y, True)
    fcx["r"] = pass_x(yr, c_x["r"])
    fxy["r"] = pass_y(xr, x_y["r"])
    lo, hi = blk(cb, y2, x, 0), blk(cb, y2, x, 1)
    c_x["2"] = [send(lo, lo, XR), send(hi, hi, XL)]
    c_x["3"] = [send(hi, hi, XR), send(lo, lo, XL)]
    partial(y)
    fxy["2"] = pass_y(x2, x_y["2"])
    got(fcx["l"])
    forward(yl)
    fcx["2"] = pass_x(y2, c_x["2"])
    weights(yl, False)
    partial(yl)
    got(fcx["r"])
    forward(yr)
    weights(yr, False)
    partial(yr)
    got(c_x["3"])
    got(fcx["2"])
    for name in ("me", "l", "r", "2"):
        got(fxy[name])
    forward(y2)
    partial(y2)

    xw = lambda k: cols(k, FX)
    h1 = [send(g.at[y2, 0:64, :], ra.at[0], YR), send(g.at[y2, 64:128, :], ra.at[1], YL)]
    h2 = [send(g.at[:, 128:192, xw(x2)], re.at[0], XR), send(g.at[:, 192:256, xw(x2)], re.at[1], XL)]
    h1b = [send(g.at[yr, 64:128, :], rb.at[0, 64:128, :], YR),
           send(g.at[yl, 0:64, :], rb.at[1, 0:64, :], YL)]
    h2b = [send(g.at[:, 192:256, xw(xr)], rf.at[0, :, 64:128, :], XR),
           send(g.at[:, 128:192, xw(xl)], rf.at[1, :, 0:64, :], XL)]

    down = ([(0, 4), (1, 3), (0, 3), (1, 2), (0, 2), (1, 1), (0, 1)],
            [(1, 4), (0, 3), (1, 3), (0, 2), (1, 2), (0, 1), (1, 1)])
    todo = []
    for i in range(7):
        for way in range(2):
            u, k = down[way][i]
            todo.append((u, k if way == 0 else -k))
    todo += [(0, 0), (1, 0)]
    own, other = cols(c, HB), cols(o, HB)
    wsum = {}
    for u, k in todo:
        az = step(z, k, NZ)
        rhs = (xb, cb)[u][y2, :, cols(az, DZ)]
        gs[u, az] = (gt[u, az, other, :] + nn(tr[u, other, :], rhs)).astype(BF16)
        wsum[u, k % NZ] = send(gs.at[u, az], pb.at[u, az], PC)
        gt[u, az, own, :] = gt[u, az, own, :] + nn(tr[u, own, :], rhs)

    gz = [[], []]

    def total(u, k):
        az = step(z, k, NZ)
        wsum[u, k % NZ].wait_recv()
        return gt[u, az, own, :] + pb[u, az].astype(F32)

    def gsend(way, i):
        u, k = down[way][i]
        value = total(u, k if way == 0 else -k)
        if i >= 2:
            gz[way][i - 2].wait_recv()
            value = value + rz[way, i - 2].astype(F32)
        sz[way, i] = value.astype(BF16)
        gz[way].append(send(sz.at[way, i], rz.at[way, i], (ZR, ZL)[way]))

    for i in range(3):
        for way in range(2):
            gsend(way, i)
    h1[0].wait_recv()
    sb[0] = (g[yr, 0:64, :].astype(F32) + ra[0].astype(F32)).astype(BF16)
    h1c = [send(sb.at[0], rb.at[0, 0:64, :], YR)]
    h1[1].wait_recv()
    sb[1] = (g[yl, 64:128, :].astype(F32) + ra[1].astype(F32)).astype(BF16)
    h1c.append(send(sb.at[1], rb.at[1, 64:128, :], YL))
    h2[0].wait_recv()
    sf[0] = (g[:, 128:192, xw(xr)].astype(F32) + re[0].astype(F32)).astype(BF16)
    h2c = [send(sf.at[0], rf.at[0, :, 0:64, :], XR)]
    h2[1].wait_recv()
    sf[1] = (g[:, 192:256, xw(xl)].astype(F32) + re[1].astype(F32)).astype(BF16)
    h2c.append(send(sf.at[1], rf.at[1, :, 64:128, :], XL))
    for i in range(3, 7):
        for way in range(2):
            gsend(way, i)

    got(h1b)
    got(h1c)
    for k in range(NX):
        s = slice(k * FX, (k + 1) * FX)
        q1[k] = g[y, 0:128, s].astype(F32) + rb[0, :, s].astype(F32) + rb[1, :, s].astype(F32)
    sd[0] = q1[x2].astype(BF16)
    sd[1, 64:128] = q1[xr, 64:128, :].astype(BF16)
    sd[2, 0:64] = q1[xl, 0:64, :].astype(BF16)
    v1 = [send(sd.at[0, 0:64, :], rc.at[0], XR), send(sd.at[0, 64:128, :], rc.at[1], XL)]
    v1b = [send(sd.at[1, 64:128, :], rd.at[0, 64:128, :], XR),
           send(sd.at[2, 0:64, :], rd.at[1, 0:64, :], XL)]
    got(h2b)
    got(h2c)
    q2[...] = g[:, 128:256, xw(x)].astype(F32) + rf[0].astype(F32) + rf[1].astype(F32)
    sh[0] = q2[y2].astype(BF16)
    sh[1, 64:128] = q2[yr, 64:128, :].astype(BF16)
    sh[2, 0:64] = q2[yl, 0:64, :].astype(BF16)
    v2 = [send(sh.at[0, 0:64, :], rg.at[0], YR), send(sh.at[0, 64:128, :], rg.at[1], YL)]
    v2b = [send(sh.at[1, 64:128, :], rh.at[0, 64:128, :], YR),
           send(sh.at[2, 0:64, :], rh.at[1, 0:64, :], YL)]

    v1[0].wait_recv()
    sd[1, 0:64] = (q1[xr, 0:64, :] + rc[0].astype(F32)).astype(BF16)
    v1c = [send(sd.at[1, 0:64, :], rd.at[0, 0:64, :], XR)]
    v1[1].wait_recv()
    sd[2, 64:128] = (q1[xl, 64:128, :] + rc[1].astype(F32)).astype(BF16)
    v1c.append(send(sd.at[2, 64:128, :], rd.at[1, 64:128, :], XL))
    v2[0].wait_recv()
    sh[1, 0:64] = (q2[yr, 0:64, :] + rg[0].astype(F32)).astype(BF16)
    v2c = [send(sh.at[1, 0:64, :], rh.at[0, 0:64, :], YR)]
    v2[1].wait_recv()
    sh[2, 64:128] = (q2[yl, 64:128, :] + rg[1].astype(F32)).astype(BF16)
    v2c.append(send(sh.at[2, 64:128, :], rh.at[1, 64:128, :], YL))

    scale = 1.0 / 128.0
    ops = []
    for u, out in ((0, ug_out), (1, dg_out)):
        way = 1 - u
        gz[0][6 - u].wait_recv()
        gz[1][5 + u].wait_recv()
        value = total(u, 0) + rz[0, 6 - u].astype(F32) + rz[1, 5 + u].astype(F32)
        gt[u, z, own, :] = (value * scale).T
        for i, (ay, where) in enumerate(((y2, Y2), (yr, YR), (yl, YL))):
            rows = pl.ds(pl.multiple_of(c * HB + ay * RY, RY), RY)
            fs_s[u, i] = gt[u, z, rows, :].astype(BF16)
            ops.append(send(fs_s.at[u, i], fs_r.at[u, i], where))
        rows = pl.ds(pl.multiple_of(c * HB + y * RY, RY), RY)
        out[:, cols(y, HB)] = gt[u, z, rows, :]

    got(v1b)
    got(v1c)
    first = q1[x] + rd[0].astype(F32) + rd[1].astype(F32)
    q1[0] = first
    got(v2b)
    got(v2c)
    second = q2[y] + rh[0].astype(F32) + rh[1].astype(F32)
    q1[1] = second
    lane = cols(o, 256)
    fp[0:128] = q1[0, :, lane].astype(BF16)
    fp[128:256] = q1[1, :, lane].astype(BF16)
    last = send(fp, rp, PC)
    lane = cols(c, 256)
    row = pl.multiple_of(c * TB, TB)
    ig_out[pl.ds(row, 128), :] = q1[0, :, lane].astype(BF16)
    ig_out[pl.ds(row + 128, 128), :] = q1[1, :, lane].astype(BF16)
    n = 0
    for u, out in ((0, ug_out), (1, dg_out)):
        for i, ay in enumerate((y2, yl, yr)):
            ops[n].wait_recv()
            n += 1
            out[:, cols(ay, HB)] = fs_r[u, i].astype(F32)
    last.wait_recv()
    ig_out[cols(o, TB), :] = rp[...]
    for copy in sent:
        copy.wait_send()


def per_device(normed_input, cotangent, up_weight, down_weight):
    bf = lambda *s: pltpu.VMEM(s, BF16)
    f4 = lambda *s: pltpu.VMEM(s, F32)
    any_spec = pl.BlockSpec(memory_space=pl.ANY)
    vmem = pl.BlockSpec(memory_space=pltpu.VMEM)
    ig, ug, dg = pl.pallas_call(
        kernel,
        out_shape=(
            jax.ShapeDtypeStruct((2 * TB, 256), BF16),
            jax.ShapeDtypeStruct((RY, 4 * HB), F32),
            jax.ShapeDtypeStruct((RY, 4 * HB), F32),
        ),
        in_specs=[any_spec] * 4,
        out_specs=(vmem,) * 3,
        scratch_shapes=[
            bf(NY, TB, D), bf(NY, TB, D),
            bf(2, 2, D, HB),
            bf(TB, 256), bf(TB, 256),
            bf(2, RY, 4 * HB),
            bf(TB, 2 * HB),
            bf(2, 2 * HB, TB),
            f4(2, NZ, 2 * HB, DZ),
            bf(2, NZ, HB, DZ), bf(2, NZ, HB, DZ),
            bf(2, 7, HB, DZ), bf(2, 7, HB, DZ),
            bf(2, 3, RY, HB), bf(2, 3, RY, HB),
            bf(NY, TB, D),
            bf(2, 64, D), bf(2, 128, D), bf(2, 64, D),
            f4(NX, 128, FX),
            bf(2, 64, FX), bf(2, 128, FX), bf(3, 128, FX),
            bf(2, NY, 64, FX), bf(2, NY, 128, FX), bf(2, NY, 64, FX),
            f4(NY, 128, FX),
            bf(2, 64, FX), bf(2, 128, FX), bf(3, 128, FX),
            bf(TB, 256), bf(TB, 256),
            pltpu.SemaphoreType.DMA((8,)),
            pltpu.SemaphoreType.DMA((COPIES,)),
            pltpu.SemaphoreType.DMA((COPIES,)),
        ],
        compiler_params=pltpu.CompilerParams(
            collective_id=0, has_side_effects=True, vmem_limit_bytes=60 * 1024 * 1024
        ),
    )(normed_input, cotangent, up_weight, down_weight.T)
    return ig, ug, dg.T


def solution(mesh):
    return jax.shard_map(
        per_device, mesh=mesh,
        in_specs=(P("fs", "tp"), P("fs", "tp"), P("fs", "tp"), P("tp", "fs")),
        out_specs=(P("fs", "tp"), P("fs", "tp"), P("tp", "fs")),
        check_vma=False,
    )
```

time: 337 us -> 107 us (0.32)
  waiting for transfers between devices: 257 us -> 0 us
  Pallas kernels: 0 us -> 103 us
  blocking collectives: 24.7 us -> 0 us
  matrix products: 23.9 us -> 0 us
  between operations: 14.2 us -> 0.65 us
  starting transfers between devices: 5.23 us -> 0 us
  other arithmetic: 4.57 us -> 0 us
    all_gather x3 -> x0, waiting for transfers between devices: 120 us -> none  [the longest x2 102 us: whole_of(): value = lax.all_gather(value, axis, axis=dim, tiled=True)]
    reduce_scatter x3 -> x0, waiting for transfers between devices: 115 us -> none  [the longest x2 67.9 us: sum_by_axis(): subtotal = lax.psum_scatter(subtotal, axis, scatter_dimension=0, tiled=True)]
    pallas_call x0 -> x1, Pallas kernels: none -> 103 us  [per_device(): pl.pallas_call(kernel, out_shape=(jax.ShapeDtypeStruct((2 * TB, 256), BF1...]
    all_gather x2 -> x0, blocking collectives: 24.7 us -> none  [whole_of(): value = lax.all_gather(value, axis, axis=dim, tiled=True)]
    dot_general x5 -> x0, matrix products: 23.9 us -> none  [the longest x2 9.85 us: right_product(): lax.dot_general(left, right, (((1,), (1,)), ((), ())), preferred_element_...]
    unnamed x8 -> x0, waiting for transfers between devices: 22 us -> none
    all_to_all x1 -> x0, starting transfers between devices: 4.98 us -> none  [sent_and_summed(): lax.all_to_all(pieces, axis, split_axis=0, concat_axis=0, tiled=True)]
  transfers between devices with their start and end apart: 8 -> 0, of which waited for: 7 -> 0; matrix products, arithmetic and copies ran while one was open for 9% -> 0% of each run, Pallas kernels for 0% -> 0%
where the time goes in v1:
time: 107 us
  Pallas kernels  103 us (96%)
  local copies, waits for them, and re-layouts  3.46 us (3%)
    pallas_call x1, Pallas kernels, per_device(): pl.pallas_call(kernel, out_shape=(jax.ShapeDtypeStruct((2 * TB, 256), BF1...  103 us
    unnamed x7, local copies, waits for them, and re-layouts  3.46 us

profile of v1, /device:TPU:1, one launch (start us, length us, event | category | flops | bytes accessed | tf_op | source)
XLA Modules:
  0.0 106.7 jit_solution(13703998167657008721)
XLA Ops:
  0.6 102.6 %shard_map.67 = (bf16[512,256]{1,0:T(8,128)(2,1)}, f32[64,1024]{1,0:T(8,128)}, f32[64,1024]{1,0:T(8,128)}) custom-call(bf16[512,256]{1,0:T(8,128)(2,1)} %x_in.1, bf16[512,256]{1,0:T(8,128)(2,1)} %c_in.1, bf16[64,1024]{1,0:T(8,128)(2,1)} %up_in.1, bf16[64,1024]{1,0:T(8,128)(2,1)} %bitcast.3), custom_call_target="tpu_custom_call" | custom-call | tf_op jit(solution)/shard_map/pallas_call | solution.py:394
  103.2 0.0 copy-start.1
  103.2 1.7 %copy.10 = bf16[512,256]{1,0:T(8,128)(2,1)} copy(bf16[512,256]{1,0:T(8,128)(2,1)} %get-tuple-element.12) | data formatting | bytes 524288
  104.9 0.0 copy-done.1
  104.9 0.0 copy-start
  104.9 0.7 copy.11
  105.6 0.3 copy-done
  106.0 0.7 copy.12
Async XLA Ops:
  103.2 1.7 %copy-start.1 = (f32[64,1024]{1,0:T(8,128)S(1)}, f32[64,1024]{1,0:T(8,128)}, u32[]{:S(2)}) copy-start(f32[64,1024]{1,0:T(8,128)} %get-tuple-element.13) | copy-start | bytes 786436
  104.9 1.0 copy-start

commit v2 on v1

v2 whole, which is shorter than its diff:
```python
import jax
import jax.numpy as jnp
from jax import lax
from jax.experimental import pallas as pl
from jax.experimental.pallas import tpu as pltpu
from jax.sharding import PartitionSpec as P

NX, NY, NZ = 4, 4, 8
D = 2048
TB = 256
FX = 512
HB = 256
DZ = 256
RY = 64
HALF = TB // 2
QUART = TB // 4
COPIES = 160
MESH = pl.DeviceIdType.MESH
BF16, F32 = jnp.bfloat16, jnp.float32


def nn(a, b):
    return lax.dot_general(a, b, (((1,), (0,)), ((), ())), preferred_element_type=F32)


def nt(a, b):
    return lax.dot_general(a, b, (((1,), (1,)), ((), ())), preferred_element_type=F32)


def kernel(
    x_in, c_in, up_in, dn_in, ow, og,
    xb, cb, w, xs, cs, uv, pg, tr, acc, gt, gs, pb, rz, sz, fs_s, g,
    ra, rb, sb, q1, rc, rd, sd, re, rf, sf, q2, rg, rh, sh, fp,
    lsem, ssem, rsem,
):
    fs, tp = lax.axis_index("fs"), lax.axis_index("tp")
    z, y = lax.div(fs, NY), lax.rem(fs, NY)
    x, c = lax.div(tp, 2), lax.rem(tp, 2)
    o = 1 - c
    step = lambda a, k, n: lax.rem(a + (k % n), n)
    xr, xl, x2 = step(x, 1, NX), step(x, -1, NX), step(x, 2, NX)
    yr, yl, y2 = step(y, 1, NY), step(y, -1, NY), step(y, 2, NY)
    at = lambda ax, ay, az, ac: (az * NY + ay, ax * 2 + ac)
    XR, XL = at(xr, y, z, c), at(xl, y, z, c)
    YR, YL, Y2 = at(x, yr, z, c), at(x, yl, z, c), at(x, y2, z, c)
    ZR, ZL = at(x, y, step(z, 1, NZ), c), at(x, y, step(z, -1, NZ), c)
    PC = at(x, y, z, o)
    ME, L, R, OPP = range(4)

    ids = iter(range(COPIES))
    sent = []

    def send(src, dst, where):
        i = next(ids)
        copy = pltpu.make_async_remote_copy(
            src_ref=src, dst_ref=dst, send_sem=ssem.at[i], recv_sem=rsem.at[i],
            device_id=where, device_id_type=MESH,
        )
        copy.start()
        sent.append(copy)
        return copy

    def got(ops):
        for op in ops:
            op.wait_recv()

    def cols(k, n):
        return pl.ds(pl.multiple_of(k * n, n), n)

    mine = pl.ds(pl.multiple_of(x * FX + c * 256, 256), 256)
    wrow = pl.ds(pl.multiple_of(z * DZ + y * RY, RY), RY)
    loads = []
    for i, (src, dst) in enumerate((
        (c_in.at[cols(o, TB), :], cs),
        (x_in.at[cols(o, TB), :], xs),
        (up_in, uv.at[0]),
        (dn_in, uv.at[1]),
        (c_in.at[cols(c, TB), :], cb.at[0:TB, mine]),
        (x_in.at[cols(c, TB), :], xb.at[0:TB, mine]),
        (up_in.at[:, cols(y, HB)], w.at[0, wrow, 0:HB]),
        (dn_in.at[:, cols(y, HB)], w.at[1, wrow, 0:HB]),
    )):
        copy = pltpu.make_async_copy(src, dst, lsem.at[i])
        copy.start()
        loads.append(copy)

    barrier = pltpu.get_barrier_semaphore()
    peers = (XR, XL, YR, YL, Y2, ZR, ZL, PC)
    for peer in peers:
        pl.semaphore_signal(barrier, inc=1, device_id=peer, device_id_type=MESH)
    pl.semaphore_wait(barrier, len(peers))

    loads[0].wait()
    cop = send(cs, cb.at[0:TB, mine], PC)
    loads[1].wait()
    xop = send(xs, xb.at[0:TB, mine], PC)
    loads[2].wait()
    loads[3].wait()
    wops = []
    for ay, where in ((y2, Y2), (yr, YR), (yl, YL)):
        for u in range(2):
            wops.append(send(uv.at[u, :, cols(ay, HB)], w.at[u, wrow, 0:HB], where))

    def blk(buf, slot, ax, half=None):
        if half is None:
            return buf.at[slot * TB:(slot + 1) * TB, cols(ax, FX)]
        return buf.at[slot * TB + half * HALF:slot * TB + (half + 1) * HALF, cols(ax, FX)]

    def over_x(buf, slot, ax):
        ref = blk(buf, slot, ax)
        return [send(ref, ref, XR), send(ref, ref, XL)]

    def over_y(buf, ax):
        ref = blk(buf, ME, ax)
        return [send(ref, blk(buf, L, ax), YR), send(ref, blk(buf, R, ax), YL)]

    def pass_x(buf, slot, ops):
        ops[0].wait_recv()
        a = blk(buf, slot, xl, 0)
        first = send(a, a, XR)
        ops[1].wait_recv()
        b = blk(buf, slot, xr, 1)
        return [first, send(b, b, XL)]

    def pass_y(buf, ax, ops):
        ops[0].wait_recv()
        first = send(blk(buf, L, ax, 0), blk(buf, OPP, ax, 0), YR)
        ops[1].wait_recv()
        return [first, send(blk(buf, R, ax, 1), blk(buf, OPP, ax, 1), YL)]

    loads[4].wait()
    loads[5].wait()
    cop.wait_recv()
    c_y = over_y(cb, x)
    xop.wait_recv()
    x_x = over_x(xb, ME, x)
    x_y = {"me": over_y(xb, x)}
    c_x = {"me": over_x(cb, ME, x)}

    loads[6].wait()
    loads[7].wait()
    got(wops)

    wz = [[], []]
    wpc = []
    order = ([(0, 0), (1, 0), (0, 1), (1, 1), (0, 2), (1, 2), (0, 3)],
             [(1, 0), (0, 0), (1, 1), (0, 1), (1, 2), (0, 2), (1, 3)])

    def wsend(way, i):
        u, k = order[way][i]
        ref = w.at[u, cols(step(z, -k if way == 0 else k, NZ), DZ), 0:HB]
        wz[way].append(send(ref, ref, (ZR, ZL)[way]))

    def wpair(u, k):
        rows = cols(step(z, k, NZ), DZ)
        wpc.append(send(w.at[u, rows, 0:HB], w.at[u, rows, HB:2 * HB], PC))

    for i in range(2):
        for way in range(2):
            wsend(way, i)
    for u in range(2):
        wpair(u, 0)

    def warrive(i):
        for way in range(2):
            wz[way][i].wait_recv()
            u, k = order[way][i]
            if i + 2 < 7:
                wsend(way, i + 2)
            wpair(u, -(k + 1) if way == 0 else k + 1)

    fx = pass_x(xb, ME, x_x)
    warrive(0)
    fc = pass_y(cb, x, c_y)
    x_y["l"] = over_y(xb, xl)
    x_y["r"] = over_y(xb, xr)
    warrive(1)
    fcx = {"me": pass_x(cb, ME, c_x["me"])}
    c_x["l"] = over_x(cb, L, x)
    c_x["r"] = over_x(cb, R, x)
    warrive(2)
    got(fx)
    x_y["2"] = over_y(xb, x2)
    warrive(3)
    fxy = {"me": pass_y(xb, x, x_y["me"])}
    got(fc)
    warrive(4)
    warrive(5)
    fcx["l"] = pass_x(cb, L, c_x["l"])
    fxy["l"] = pass_y(xb, xl, x_y["l"])
    warrive(6)
    got(fcx["me"])
    got(wpc)

    def forward(slot, pre=None, act_grad=None):
        rows = slice(slot * TB, (slot + 1) * TB)
        for h in range(2):
            s = slice(h * HB, (h + 1) * HB)
            pre = nn(xb[rows], w[0, :, s])
            act_grad = nn(cb[rows], w[1, :, s])
            finish(slot, s, pre, act_grad)

    def finish(slot, s, pre, act_grad):
        rows = slice(slot * TB, (slot + 1) * TB)
        rect = jnp.maximum(pre, 0.0)
        grad = 2.0 * rect * act_grad
        pg[rows, s] = grad.astype(BF16)
        tr[0, s, rows] = grad.T.astype(BF16)
        tr[1, s, rows] = (rect * rect).T.astype(BF16)

    def partial(lo, hi):
        rows = slice(lo * TB, hi * TB)

        @pl.loop(0, NZ, unroll=2)
        def _(k):
            lane = cols(k, DZ)
            g[rows, lane] = nt(pg[rows, :], w[0, lane, :]).astype(BF16)

    forward(ME)
    fcx["r"] = pass_x(cb, R, c_x["r"])
    c2 = [send(blk(cb, OPP, x, h), blk(cb, OPP, x, h), (XR, XL)[h]) for h in range(2)]
    c3 = [send(blk(cb, OPP, x, 1 - h), blk(cb, OPP, x, 1 - h), (XR, XL)[h]) for h in range(2)]
    partial(ME, L)
    fxy["r"] = pass_y(xb, xr, x_y["r"])
    fxy["2"] = pass_y(xb, x2, x_y["2"])
    got(fcx["l"])
    forward(L)
    fcx["2"] = pass_x(cb, OPP, c2)
    got(fcx["r"])
    forward(R)
    partial(L, OPP)

    def part(slot, r, n, lane=slice(None)):
        return g.at[slot * TB + r:slot * TB + r + n, lane]

    h1b = [send(part(R, 64, 64), rb.at[0, 64:128, :], YR),
           send(part(L, 0, 64), rb.at[1, 0:64, :], YL)]
    h2, h2b = {}, {}
    far, right, left = cols(x2, FX), cols(xr, FX), cols(xl, FX)

    def first_x(slot):
        h2[slot] = [send(part(slot, 128, 64, far), re.at[0, slot], XR),
                    send(part(slot, 192, 64, far), re.at[1, slot], XL)]

    def next_x(slot):
        h2b[slot] = [send(part(slot, 192, 64, right), rf.at[0, slot, 64:128], XR),
                     send(part(slot, 128, 64, left), rf.at[1, slot, 0:64], XL)]

    def last_x(slot):
        h2[slot][0].wait_recv()
        sf[0, slot] = (part(slot, 128, 64, right)[...].astype(F32) + re[0, slot].astype(F32)).astype(BF16)
        h2b[slot].append(send(sf.at[0, slot], rf.at[0, slot, 0:64], XR))
        h2[slot][1].wait_recv()
        sf[1, slot] = (part(slot, 192, 64, left)[...].astype(F32) + re[1, slot].astype(F32)).astype(BF16)
        h2b[slot].append(send(sf.at[1, slot], rf.at[1, slot, 64:128], XL))

    for slot in (ME, L, R):
        first_x(slot)
    for slot in (ME, L, R):
        next_x(slot)

    for u, buf in ((0, xb), (1, cb)):
        @pl.loop(0, NZ, unroll=2)
        def _(k):
            gt[u, k] = nn(tr[u, :, 0:3 * TB], buf[0:3 * TB, cols(k, DZ)])

    orow = slice(OPP * TB, OPP * TB + TB)
    got(c3)
    got(fcx["2"])
    for h in range(2):
        s = slice(h * HB, (h + 1) * HB)
        acc[1, :, s] = nn(cb[orow], w[1, :, s])
    got(fxy["me"] + fxy["l"] + fxy["r"])
    for n, ax in enumerate((x, xl, xr)):
        lane = cols(ax, FX)
        term = nn(xb[orow, lane], w[0, lane, :])
        acc[0] = term if n == 0 else acc[0] + term
    got(fxy["2"])
    pre = acc[0] + nn(xb[orow, far], w[0, far, :])
    finish(OPP, slice(0, 2 * HB), pre, acc[1])

    down = ([(0, 4), (1, 3), (0, 3), (1, 2), (0, 2), (1, 1), (0, 1)],
            [(1, 4), (0, 3), (1, 3), (0, 2), (1, 2), (0, 1), (1, 1)])
    todo = []
    for i in range(7):
        for way in range(2):
            u, k = down[way][i]
            todo.append((u, k if way == 0 else -k))
    todo += [(0, 0), (1, 0)]
    wsum = {}

    def chunk(u, k):
        az = step(z, k, NZ)
        value = gt[u, az] + nn(tr[u, :, 3 * TB:], (xb, cb)[u][orow, cols(az, DZ)])
        gs[u, az] = value[HB:].astype(BF16)
        wsum[u, k % NZ] = send(gs.at[u, az], pb.at[u, az], PC)
        gt[u, az, 0:HB] = value[:HB]

    gz = [[], []]

    def total(u, k):
        az = step(z, k, NZ)
        wsum[u, k % NZ].wait_recv()
        return gt[u, az, 0:HB] + pb[u, az].astype(F32)

    def gsend(i):
        for way in range(2):
            u, k = down[way][i]
            value = total(u, k if way == 0 else -k)
            if i >= 2:
                gz[way][i - 2].wait_recv()
                value = value + rz[way, i - 2].astype(F32)
            sz[way, i] = value.astype(BF16)
            gz[way].append(send(sz.at[way, i], rz.at[way, i], (ZR, ZL)[way]))

    for u, k in todo[:4]:
        chunk(u, k)
    gsend(0)
    partial(OPP, OPP + 1)
    h1 = [send(part(OPP, 0, 64), ra.at[0], YR), send(part(OPP, 64, 64), ra.at[1], YL)]
    first_x(OPP)
    next_x(OPP)
    gsend(1)
    for slot in (ME, L, R):
        last_x(slot)
    for u, k in todo[4:]:
        chunk(u, k)
    gsend(2)
    h1[0].wait_recv()
    sb[0] = (part(R, 0, 64)[...].astype(F32) + ra[0].astype(F32)).astype(BF16)
    h1c = [send(sb.at[0], rb.at[0, 0:64, :], YR)]
    h1[1].wait_recv()
    sb[1] = (part(L, 64, 64)[...].astype(F32) + ra[1].astype(F32)).astype(BF16)
    h1c.append(send(sb.at[1], rb.at[1, 64:128, :], YL))
    last_x(OPP)
    gsend(3)
    gsend(4)

    for slot in range(4):
        got(h2b[slot])
    here = cols(x, FX)
    for slot in range(4):
        q2[slot] = (part(slot, 128, 128, here)[...].astype(F32)
                    + rf[0, slot].astype(F32) + rf[1, slot].astype(F32))
    sh[0] = q2[OPP].astype(BF16)
    sh[1, 64:128] = q2[R, 64:128, :].astype(BF16)
    sh[2, 0:64] = q2[L, 0:64, :].astype(BF16)
    v2 = [send(sh.at[0, 0:64, :], rg.at[0], YR), send(sh.at[0, 64:128, :], rg.at[1], YL)]
    v2b = [send(sh.at[1, 64:128, :], rh.at[0, 64:128, :], YR),
           send(sh.at[2, 0:64, :], rh.at[1, 0:64, :], YL)]
    got(h1b)
    got(h1c)
    for k in range(NX):
        s = slice(k * FX, (k + 1) * FX)
        q1[k] = g[0:128, s].astype(F32) + rb[0, :, s].astype(F32) + rb[1, :, s].astype(F32)
    sd[0] = q1[x2].astype(BF16)
    sd[1, 64:128] = q1[xr, 64:128, :].astype(BF16)
    sd[2, 0:64] = q1[xl, 0:64, :].astype(BF16)
    v1 = [send(sd.at[0, 0:64, :], rc.at[0], XR), send(sd.at[0, 64:128, :], rc.at[1], XL)]
    v1b = [send(sd.at[1, 64:128, :], rd.at[0, 64:128, :], XR),
           send(sd.at[2, 0:64, :], rd.at[1, 0:64, :], XL)]
    gsend(5)
    v2[0].wait_recv()
    sh[1, 0:64] = (q2[R, 0:64, :] + rg[0].astype(F32)).astype(BF16)
    v2c = [send(sh.at[1, 0:64, :], rh.at[0, 0:64, :], YR)]
    v2[1].wait_recv()
    sh[2, 64:128] = (q2[L, 64:128, :] + rg[1].astype(F32)).astype(BF16)
    v2c.append(send(sh.at[2, 64:128, :], rh.at[1, 64:128, :], YL))
    v1[0].wait_recv()
    sd[1, 0:64] = (q1[xr, 0:64, :] + rc[0].astype(F32)).astype(BF16)
    v1c = [send(sd.at[1, 0:64, :], rd.at[0, 0:64, :], XR)]
    v1[1].wait_recv()
    sd[2, 64:128] = (q1[xl, 64:128, :] + rc[1].astype(F32)).astype(BF16)
    v1c.append(send(sd.at[2, 64:128, :], rd.at[1, 64:128, :], XL))
    gsend(6)
    own, other = cols(c, 256), cols(o, 256)
    ends = []

    def finish_rows(r, value, n):
        q1[n] = value
        fp[0, r:r + 128] = q1[n, :, other].astype(BF16)
        fp[1, r:r + 128] = q1[n, :, own].astype(BF16)
        row = pl.ds(pl.multiple_of(c * TB + r, 128), 128)
        ends.append(send(fp.at[0, r:r + 128], og.at[row, :], PC))
        copy = pltpu.make_async_copy(fp.at[1, r:r + 128], og.at[row, :], lsem.at[8 + n])
        copy.start()
        return copy

    got(v1b)
    got(v1c)
    stores = [finish_rows(0, q1[x] + rd[0].astype(F32) + rd[1].astype(F32), 0)]
    got(v2b)
    got(v2c)
    stores.append(finish_rows(128, q2[ME] + rh[0].astype(F32) + rh[1].astype(F32), 1))

    scale = 1.0 / 128.0
    ops = []
    for u in range(2):
        value = total(u, 0)
        gz[0][6 - u].wait_recv()
        gz[1][5 + u].wait_recv()
        value = value + rz[0, 6 - u].astype(F32) + rz[1, 5 + u].astype(F32)
        fs_s[u] = (value * scale).T.astype(BF16)
        there = cols(y, HB)
        for ay, where in ((y2, Y2), (yr, YR), (yl, YL)):
            ops.append(send(fs_s.at[u, cols(ay, RY), :], ow.at[u, :, there], where))
        copy = pltpu.make_async_copy(fs_s.at[u, cols(y, RY), :], ow.at[u, :, there], lsem.at[10 + u])
        copy.start()
        stores.append(copy)
    got(ops)
    got(ends)
    for copy in stores:
        copy.wait()
    for copy in sent:
        copy.wait_send()


def finisher(ow, og, ig_out, ug_out, dg_out, wv, gv, fv, sem):
    loads = [pltpu.make_async_copy(ow.at[u], wv.at[u], sem.at[u]) for u in range(2)]
    loads.append(pltpu.make_async_copy(og, gv, sem.at[2]))
    for copy in loads:
        copy.start()
    stores = []
    for u, out in ((0, ug_out), (1, dg_out)):
        loads[u].wait()
        fv[u] = wv[u].astype(F32)
        stores.append(pltpu.make_async_copy(fv.at[u], out, sem.at[3 + u]))
        stores[-1].start()
    loads[2].wait()
    stores.append(pltpu.make_async_copy(gv, ig_out, sem.at[5]))
    stores[-1].start()
    for copy in stores:
        copy.wait()


def per_device(normed_input, cotangent, up_weight, down_weight):
    bf = lambda *s: pltpu.VMEM(s, BF16)
    f4 = lambda *s: pltpu.VMEM(s, F32)
    hbm = pl.BlockSpec(memory_space=pl.ANY)
    shape = jax.ShapeDtypeStruct
    ow, og = pl.pallas_call(
        kernel,
        out_shape=(shape((2, RY, 4 * HB), BF16), shape((2 * TB, 256), BF16)),
        in_specs=[hbm] * 4,
        out_specs=(hbm,) * 2,
        scratch_shapes=[
            bf(NY * TB, D), bf(NY * TB, D),
            bf(2, D, 2 * HB),
            bf(TB, 256), bf(TB, 256),
            bf(2, RY, 4 * HB),
            bf(NY * TB, 2 * HB),
            bf(2, 2 * HB, NY * TB),
            f4(2, TB, 2 * HB),
            f4(2, NZ, 2 * HB, DZ),
            bf(2, NZ, HB, DZ), bf(2, NZ, HB, DZ),
            bf(2, 7, HB, DZ), bf(2, 7, HB, DZ),
            bf(2, DZ, HB),
            bf(NY * TB, D),
            bf(2, 64, D), bf(2, 128, D), bf(2, 64, D),
            f4(NX, 128, FX),
            bf(2, 64, FX), bf(2, 128, FX), bf(3, 128, FX),
            bf(2, NY, 64, FX), bf(2, NY, 128, FX), bf(2, NY, 64, FX),
            f4(NY, 128, FX),
            bf(2, 64, FX), bf(2, 128, FX), bf(3, 128, FX),
            bf(2, TB, 256),
            pltpu.SemaphoreType.DMA((12,)),
            pltpu.SemaphoreType.DMA((COPIES,)),
            pltpu.SemaphoreType.DMA((COPIES,)),
        ],
        compiler_params=pltpu.CompilerParams(
            collective_id=0, has_side_effects=True, vmem_limit_bytes=60 * 1024 * 1024
        ),
    )(normed_input, cotangent, up_weight, down_weight.T)
    ig, ug, dg = pl.pallas_call(
        finisher,
        out_shape=(shape((2 * TB, 256), BF16), shape((RY, 4 * HB), F32), shape((RY, 4 * HB), F32)),
        in_specs=[hbm] * 2,
        out_specs=(hbm,) * 3,
        scratch_shapes=[
            bf(2, RY, 4 * HB), bf(2 * TB, 256), f4(2, RY, 4 * HB), pltpu.SemaphoreType.DMA((6,)),
        ],
    )(ow, og)
    return ig, ug, dg.T


def solution(mesh):
    return jax.shard_map(
        per_device, mesh=mesh,
        in_specs=(P("fs", "tp"), P("fs", "tp"), P("fs", "tp"), P("tp", "fs")),
        out_specs=(P("fs", "tp"), P("fs", "tp"), P("tp", "fs")),
        check_vma=False,
    )
```

time: 107 us -> 97.1 us (0.907)
  the two profiles are of different devices: /device:TPU:1 before, /device:TPU:8 now
where the time goes in v2:
time: 97.1 us; the launch traced here: 97 us
  Pallas kernels  96.4 us (99%)
    pallas_call x1, Pallas kernels, per_device(): pl.pallas_call(kernel, out_shape=(shape((2, RY, 4 * HB), BF16), shape((2...  94.5 us

profile of v2, /device:TPU:8, one launch (start us, length us, event | category | flops | bytes accessed | tf_op | source)
XLA Modules:
  0.0 97.0 jit_solution(10396281414236602714)
XLA Ops:
  0.6 94.5 %shard_map.67 = (bf16[2,64,1024]{2,1,0:T(8,128)(2,1)}, bf16[512,256]{1,0:T(8,128)(2,1)}) custom-call(bf16[512,256]{1,0:T(8,128)(2,1)} %x_in.1, bf16[512,256]{1,0:T(8,128)(2,1)} %c_in.1, bf16[64,1024]{1,0:T(8,128)(2,1)} %up_in.1, bf16[64,1024]{1,0:T(8,128)(2,1)} %bitcast.2), custom_call_target="tpu_custom_call" | custom-call | tf_op jit(solution)/shard_map/pallas_call | solution.py:441
  95.1 1.9 %shard_map.68 = (bf16[512,256]{1,0:T(8,128)(2,1)}, f32[64,1024]{1,0:T(8,128)}, f32[64,1024]{1,0:T(8,128)}) custom-call(bf16[2,64,1024]{2,1,0:T(8,128)(2,1)} %get-tuple-element.8.ow, bf16[512,256]{1,0:T(8,128)(2,1)} %get-tuple-element.9.og), custom_call_target="tpu_custom_call" | custom-call | tf_op jit(solution)/shard_map/pallas_call | solution.py:474

commit v3 on v2

v3 whole, which is shorter than its diff:
```python
import math

import jax
import jax.numpy as jnp
from jax import lax
from jax.experimental import pallas as pl
from jax.experimental.pallas import tpu as pltpu
from jax.sharding import PartitionSpec as P

NX, NY, NZ = 4, 4, 8
D = 2048
TB = 256
FX = 512
HB = 256
DZ = 256
RY = 64
HALF = TB // 2
SPLIT = (128, 112)
SENDS, RECVS = 10, 72
MESH = pl.DeviceIdType.MESH
BF16, F32 = jnp.bfloat16, jnp.float32


def nn(a, b):
    return lax.dot_general(a, b, (((1,), (0,)), ((), ())), preferred_element_type=F32)


def nt(a, b):
    return lax.dot_general(a, b, (((1,), (1,)), ((), ())), preferred_element_type=F32)


def kernel(
    x_in, c_in, up_in, dn_in, ow, og,
    xb, cb, w, xs, cs, uv, pg, tr, acc, gt, gs, pb, rz, sz, fs_s, g,
    ra, rb, sb, q1, rc, rd, sd, re, rf, sf, q2, rg, rh, sh, fp,
    lsem, ssem, rsem,
):
    fs, tp = lax.axis_index("fs"), lax.axis_index("tp")
    z, y = lax.div(fs, NY), lax.rem(fs, NY)
    x, c = lax.div(tp, 2), lax.rem(tp, 2)
    o = 1 - c
    step = lambda a, k, n: lax.rem(a + (k % n), n)
    xr, xl, x2 = step(x, 1, NX), step(x, -1, NX), step(x, 2, NX)
    yr, yl, y2 = step(y, 1, NY), step(y, -1, NY), step(y, 2, NY)
    at = lambda ax, ay, az, ac: (az * NY + ay, ax * 2 + ac)
    XR, XL = at(xr, y, z, c), at(xl, y, z, c)
    YR, YL, Y2 = at(x, yr, z, c), at(x, yl, z, c), at(x, y2, z, c)
    ZR, ZL = at(x, y, step(z, 1, NZ), c), at(x, y, step(z, -1, NZ), c)
    PC = at(x, y, z, o)
    ME, L, R, OPP = range(4)

    arrivals = iter(range(RECVS))
    groups = []
    SPAN = 4 << 20

    def size(ref):
        return math.prod(ref.shape) * 2

    def span(count):
        return xb.at[0:count // (2 * D), :]

    class Batch:
        def __init__(self):
            self.sem, self.bytes = rsem.at[next(arrivals)], 0

        def send(self, src, dst, where, small=False):
            n = size(src)
            at = next((k for k, g in enumerate(groups) if g[1] == small and g[0] + n <= SPAN), None)
            if at is None:
                at = len(groups)
                groups.append([0, small])
            groups[at][0] += n
            self.bytes += n
            pltpu.make_async_remote_copy(
                src_ref=src, dst_ref=dst, send_sem=ssem.at[at], recv_sem=self.sem,
                device_id=where, device_id_type=MESH,
            ).start()
            return self

        def wait(self):
            ref = span(self.bytes)
            pltpu.make_async_copy(ref, ref, self.sem).wait()

    def send(src, dst, where):
        return Batch().send(src, dst, where)

    def cols(k, n):
        return pl.ds(pl.multiple_of(k * n, n), n)

    mine = pl.ds(pl.multiple_of(x * FX + c * 256, 256), 256)
    wrow = pl.ds(pl.multiple_of(z * DZ + y * RY, RY), RY)
    loads = []
    for i, pairs in enumerate((
        ((c_in.at[cols(o, TB), :], cs),),
        ((x_in.at[cols(o, TB), :], xs),),
        ((up_in, uv.at[0]), (dn_in, uv.at[1])),
        ((c_in.at[cols(c, TB), :], cb.at[0:TB, mine]), (x_in.at[cols(c, TB), :], xb.at[0:TB, mine])),
        ((up_in.at[:, cols(y, HB)], w.at[0, wrow, 0:HB]),
         (dn_in.at[:, cols(y, HB)], w.at[1, wrow, 0:HB])),
    )):
        for src, dst in pairs:
            pltpu.make_async_copy(src, dst, lsem.at[i]).start()
        ref = span(sum(size(dst) for _, dst in pairs))
        loads.append(pltpu.make_async_copy(ref, ref, lsem.at[i]))

    barrier = pltpu.get_barrier_semaphore()
    peers = (XR, XL, YR, YL, Y2, ZR, ZL, PC)
    for peer in peers:
        pl.semaphore_signal(barrier, inc=1, device_id=peer, device_id_type=MESH)
    pl.semaphore_wait(barrier, len(peers))

    loads[0].wait()
    cop = send(cs, cb.at[0:TB, mine], PC)
    loads[1].wait()
    xop = send(xs, xb.at[0:TB, mine], PC)
    loads[2].wait()
    wops = Batch()
    for ay, where in ((y2, Y2), (yr, YR), (yl, YL)):
        for u in range(2):
            wops.send(uv.at[u, :, cols(ay, HB)], w.at[u, wrow, 0:HB], where, small=True)

    def blk(buf, slot, ax, lo=0, hi=TB):
        return buf.at[slot * TB + lo:slot * TB + hi, cols(ax, FX)]

    def over_x(buf, slot, ax):
        ref = blk(buf, slot, ax)
        return send(ref, ref, XR).send(ref, ref, XL)

    def over_y(buf, ax):
        ref = blk(buf, ME, ax)
        return send(ref, blk(buf, L, ax), YR).send(ref, blk(buf, R, ax), YL)

    def pass_x(buf, slot, batch, out=None):
        batch.wait()
        cut = SPLIT[0]
        a, b = blk(buf, slot, xl, 0, cut), blk(buf, slot, xr, cut)
        return (out or Batch()).send(a, a, XR).send(b, b, XL)

    def pass_y(buf, ax, batch, out=None):
        batch.wait()
        cut = SPLIT[1]
        out = out or Batch()
        out.send(blk(buf, L, ax, 0, cut), blk(buf, OPP, ax, 0, cut), YR)
        return out.send(blk(buf, R, ax, cut), blk(buf, OPP, ax, cut), YL)

    loads[3].wait()
    cop.wait()
    c_y = over_y(cb, x)
    xop.wait()
    x_x = over_x(xb, ME, x)
    x_y = {"me": over_y(xb, x)}
    c_x = {"me": over_x(cb, ME, x)}

    loads[4].wait()
    wops.wait()

    wz = []
    wpc = Batch()
    order = ([(0, 0), (1, 0), (0, 1), (1, 1), (0, 2), (1, 2), (0, 3)],
             [(1, 0), (0, 0), (1, 1), (0, 1), (1, 2), (0, 2), (1, 3)])

    def wsend(i):
        batch = Batch()
        for way in range(2):
            u, k = order[way][i]
            ref = w.at[u, cols(step(z, -k if way == 0 else k, NZ), DZ), 0:HB]
            batch.send(ref, ref, (ZR, ZL)[way])
        wz.append(batch)

    def wpair(u, k):
        rows = cols(step(z, k, NZ), DZ)
        wpc.send(w.at[u, rows, 0:HB], w.at[u, rows, HB:2 * HB], PC)

    wsend(0)
    wsend(1)
    for u in range(2):
        wpair(u, 0)

    def warrive(i):
        wz[i].wait()
        if i + 2 < 7:
            wsend(i + 2)
        for way in range(2):
            u, k = order[way][i]
            wpair(u, -(k + 1) if way == 0 else k + 1)

    fx = pass_x(xb, ME, x_x)
    warrive(0)
    fc = pass_y(cb, x, c_y)
    x_y["l"] = over_y(xb, xl)
    x_y["r"] = over_y(xb, xr)
    warrive(1)
    fcx = {"me": pass_x(cb, ME, c_x["me"])}
    c_x["l"] = over_x(cb, L, x)
    c_x["r"] = over_x(cb, R, x)
    warrive(2)
    fx.wait()
    x_y["2"] = over_y(xb, x2)
    warrive(3)
    fxy = pass_y(xb, x, x_y["me"])
    fc.wait()
    warrive(4)
    warrive(5)
    fcx["l"] = pass_x(cb, L, c_x["l"])
    pass_y(xb, xl, x_y["l"], fxy)
    warrive(6)
    fcx["me"].wait()
    wpc.wait()

    def forward(slot):
        rows = slice(slot * TB, (slot + 1) * TB)
        for h in range(2):
            s = slice(h * HB, (h + 1) * HB)
            pre = nn(xb[rows], w[0, :, s])
            act_grad = nn(cb[rows], w[1, :, s])
            finish(slot, s, pre, act_grad)

    def finish(slot, s, pre, act_grad):
        rows = slice(slot * TB, (slot + 1) * TB)
        rect = jnp.maximum(pre, 0.0)
        grad = 2.0 * rect * act_grad
        pg[rows, s] = grad.astype(BF16)
        tr[0, s, rows] = grad.T.astype(BF16)
        tr[1, s, rows] = (rect * rect).T.astype(BF16)

    def partial(lo, hi):
        rows = slice(lo * TB, hi * TB)

        @pl.loop(0, NZ, unroll=2)
        def _(k):
            lane = cols(k, DZ)
            g[rows, lane] = nt(pg[rows, :], w[0, lane, :]).astype(BF16)

    forward(ME)
    fcx["r"] = pass_x(cb, R, c_x["r"])
    lo, hi = blk(cb, OPP, x, 0, HALF), blk(cb, OPP, x, HALF)
    c2 = send(lo, lo, XR).send(hi, hi, XL)
    c3 = send(hi, hi, XR).send(lo, lo, XL)
    partial(ME, L)
    pass_y(xb, xr, x_y["r"], fxy)
    fxy2 = pass_y(xb, x2, x_y["2"])
    fcx["l"].wait()
    forward(L)
    fcx["r"].wait()
    forward(R)
    fcx["2"] = pass_x(cb, OPP, c2)
    partial(L, OPP)

    def part(slot, r, n, lane=slice(None)):
        return g.at[slot * TB + r:slot * TB + r + n, lane]

    h1b = Batch()
    h1b.send(part(R, 64, 64), rb.at[0, 64:128, :], YR)
    h1b.send(part(L, 0, 64), rb.at[1, 0:64, :], YL)
    far, right, left = cols(x2, FX), cols(xr, FX), cols(xl, FX)
    h2, h2b = {}, Batch()

    def first_x(slots):
        batch = Batch()
        for slot in slots:
            batch.send(part(slot, 128, 64, far), re.at[0, slot], XR)
            batch.send(part(slot, 192, 64, far), re.at[1, slot], XL)
            h2[slot] = batch
        return batch

    def next_x(slot):
        h2b.send(part(slot, 192, 64, right), rf.at[0, slot, 64:128], XR)
        h2b.send(part(slot, 128, 64, left), rf.at[1, slot, 0:64], XL)

    def last_x(slot):
        sf[0, slot] = (part(slot, 128, 64, right)[...].astype(F32) + re[0, slot].astype(F32)).astype(BF16)
        h2b.send(sf.at[0, slot], rf.at[0, slot, 0:64], XR)
        sf[1, slot] = (part(slot, 192, 64, left)[...].astype(F32) + re[1, slot].astype(F32)).astype(BF16)
        h2b.send(sf.at[1, slot], rf.at[1, slot, 64:128], XL)

    h2early = first_x((ME, L, R))
    for slot in (ME, L, R):
        next_x(slot)

    for u, buf in ((0, xb), (1, cb)):
        @pl.loop(0, NZ, unroll=2)
        def _(k):
            gt[u, k] = nn(tr[u, :, 0:3 * TB], buf[0:3 * TB, cols(k, DZ)])

    orow = slice(OPP * TB, OPP * TB + TB)
    c3.wait()
    fcx["2"].wait()
    for h in range(2):
        s = slice(h * HB, (h + 1) * HB)
        acc[1, :, s] = nn(cb[orow], w[1, :, s])
    fxy.wait()
    for n, ax in enumerate((x, xl, xr)):
        lane = cols(ax, FX)
        term = nn(xb[orow, lane], w[0, lane, :])
        acc[0] = term if n == 0 else acc[0] + term
    fxy2.wait()
    pre = acc[0] + nn(xb[orow, far], w[0, far, :])
    finish(OPP, slice(0, 2 * HB), pre, acc[1])

    down = ([(0, 4), (1, 3), (0, 3), (1, 2), (0, 2), (1, 1), (0, 1)],
            [(1, 4), (0, 3), (1, 3), (0, 2), (1, 2), (0, 1), (1, 1)])
    todo = []
    for i in range(7):
        for way in range(2):
            u, k = down[way][i]
            todo.append((u, k if way == 0 else -k))
    todo += [(0, 0), (1, 0)]
    wsum = []

    def chunks(i):
        batch = Batch()
        for u, k in todo[2 * i:2 * i + 2]:
            az = step(z, k, NZ)
            value = gt[u, az] + nn(tr[u, :, 3 * TB:], (xb, cb)[u][orow, cols(az, DZ)])
            gs[u, az] = value[HB:].astype(BF16)
            batch.send(gs.at[u, az], pb.at[u, az], PC)
            gt[u, az, 0:HB] = value[:HB]
        wsum.append(batch)

    gz = []

    def total(u, k):
        az = step(z, k, NZ)
        return gt[u, az, 0:HB] + pb[u, az].astype(F32)

    def gsend(i):
        wsum[i].wait()
        if i >= 2:
            gz[i - 2].wait()
        batch = Batch()
        for way in range(2):
            u, k = down[way][i]
            value = total(u, k if way == 0 else -k)
            if i >= 2:
                value = value + rz[way, i - 2].astype(F32)
            sz[way, i] = value.astype(BF16)
            batch.send(sz.at[way, i], rz.at[way, i], (ZR, ZL)[way])
        gz.append(batch)

    chunks(0)
    chunks(1)
    gsend(0)
    partial(OPP, OPP + 1)
    h1 = []
    for r in (0, 32):
        h1.append(send(part(OPP, r, 32), ra.at[0, r:r + 32], YR)
                  .send(part(OPP, 64 + r, 32), ra.at[1, r:r + 32], YL))
    first_x((OPP,))
    next_x(OPP)
    gsend(1)
    h2early.wait()
    for slot in (ME, L, R):
        last_x(slot)
    chunks(2)
    gsend(2)
    chunks(3)
    chunks(4)
    def next_y(n, r):
        h1[n].wait()
        sb[0, r:r + 32] = (part(R, r, 32)[...].astype(F32) + ra[0, r:r + 32].astype(F32)).astype(BF16)
        h1b.send(sb.at[0, r:r + 32], rb.at[0, r:r + 32, :], YR)
        sb[1, r:r + 32] = (part(L, 64 + r, 32)[...].astype(F32) + ra[1, r:r + 32].astype(F32)).astype(BF16)
        h1b.send(sb.at[1, r:r + 32], rb.at[1, 64 + r:96 + r, :], YL)

    next_y(0, 0)
    gsend(3)
    h2[OPP].wait()
    last_x(OPP)
    next_y(1, 32)
    chunks(5)
    chunks(6)
    gsend(4)
    chunks(7)
    gsend(5)

    h2b.wait()
    here = cols(x, FX)
    for slot in range(4):
        q2[slot] = (part(slot, 128, 128, here)[...].astype(F32)
                    + rf[0, slot].astype(F32) + rf[1, slot].astype(F32))
    sh[0] = q2[OPP].astype(BF16)
    sh[1, 64:128] = q2[R, 64:128, :].astype(BF16)
    sh[2, 0:64] = q2[L, 0:64, :].astype(BF16)
    v2 = send(sh.at[0, 0:64, :], rg.at[0], YR).send(sh.at[0, 64:128, :], rg.at[1], YL)
    v2b = Batch()
    v2b.send(sh.at[1, 64:128, :], rh.at[0, 64:128, :], YR)
    v2b.send(sh.at[2, 0:64, :], rh.at[1, 0:64, :], YL)
    h1b.wait()
    for k in range(NX):
        s = slice(k * FX, (k + 1) * FX)
        q1[k] = g[0:128, s].astype(F32) + rb[0, :, s].astype(F32) + rb[1, :, s].astype(F32)
    sd[0] = q1[x2].astype(BF16)
    sd[1, 64:128] = q1[xr, 64:128, :].astype(BF16)
    sd[2, 0:64] = q1[xl, 0:64, :].astype(BF16)
    v1 = send(sd.at[0, 0:64, :], rc.at[0], XR).send(sd.at[0, 64:128, :], rc.at[1], XL)
    v1b = Batch()
    v1b.send(sd.at[1, 64:128, :], rd.at[0, 64:128, :], XR)
    v1b.send(sd.at[2, 0:64, :], rd.at[1, 0:64, :], XL)
    gsend(6)
    v2.wait()
    sh[1, 0:64] = (q2[R, 0:64, :] + rg[0].astype(F32)).astype(BF16)
    v2b.send(sh.at[1, 0:64, :], rh.at[0, 0:64, :], YR)
    sh[2, 64:128] = (q2[L, 64:128, :] + rg[1].astype(F32)).astype(BF16)
    v2b.send(sh.at[2, 64:128, :], rh.at[1, 64:128, :], YL)
    v1.wait()
    sd[1, 0:64] = (q1[xr, 0:64, :] + rc[0].astype(F32)).astype(BF16)
    v1b.send(sd.at[1, 0:64, :], rd.at[0, 0:64, :], XR)
    sd[2, 64:128] = (q1[xl, 64:128, :] + rc[1].astype(F32)).astype(BF16)
    v1b.send(sd.at[2, 64:128, :], rd.at[1, 64:128, :], XL)
    own, other = cols(c, 256), cols(o, 256)
    ends = Batch()
    stored = [0]

    def store(src, dst):
        pltpu.make_async_copy(src, dst, lsem.at[5]).start()
        stored[0] += size(src)

    def finish_rows(r, value, n):
        q1[n] = value
        fp[0, r:r + 128] = q1[n, :, other].astype(BF16)
        fp[1, r:r + 128] = q1[n, :, own].astype(BF16)
        row = pl.ds(pl.multiple_of(c * TB + r, 128), 128)
        ends.send(fp.at[0, r:r + 128], og.at[row, :], PC)
        store(fp.at[1, r:r + 128], og.at[row, :])

    v1b.wait()
    finish_rows(0, q1[x] + rd[0].astype(F32) + rd[1].astype(F32), 0)
    v2b.wait()
    finish_rows(128, q2[ME] + rh[0].astype(F32) + rh[1].astype(F32), 1)

    scale = 1.0 / 128.0
    ops = Batch()
    wsum[7].wait()
    gz[5].wait()
    gz[6].wait()
    for u in range(2):
        value = total(u, 0) + rz[0, 6 - u].astype(F32) + rz[1, 5 + u].astype(F32)
        fs_s[u] = (value * scale).T.astype(BF16)
        there = cols(y, HB)
        for ay, where in ((y2, Y2), (yr, YR), (yl, YL)):
            ops.send(fs_s.at[u, cols(ay, RY), :], ow.at[u, :, there], where, small=True)
        store(fs_s.at[u, cols(y, RY), :], ow.at[u, :, there])
    ops.wait()
    ends.wait()
    ref = span(stored[0])
    pltpu.make_async_copy(ref, ref, lsem.at[5]).wait()
    for k, (n, _) in enumerate(groups):
        ref = span(n)
        pltpu.make_async_copy(ref, ref, ssem.at[k]).wait()


def finisher(ow, og, ig_out, ug_out, dg_out, wv, gv, fv, sem):
    loads = [pltpu.make_async_copy(ow.at[u], wv.at[u], sem.at[u]) for u in range(2)]
    loads.append(pltpu.make_async_copy(og, gv, sem.at[2]))
    for copy in loads:
        copy.start()
    stores = []
    for u, out in ((0, ug_out), (1, dg_out)):
        loads[u].wait()
        fv[u] = wv[u].astype(F32)
        stores.append(pltpu.make_async_copy(fv.at[u], out, sem.at[3 + u]))
        stores[-1].start()
    loads[2].wait()
    stores.append(pltpu.make_async_copy(gv, ig_out, sem.at[5]))
    stores[-1].start()
    for copy in stores:
        copy.wait()


def per_device(normed_input, cotangent, up_weight, down_weight):
    bf = lambda *s: pltpu.VMEM(s, BF16)
    f4 = lambda *s: pltpu.VMEM(s, F32)
    hbm = pl.BlockSpec(memory_space=pl.ANY)
    shape = jax.ShapeDtypeStruct
    ow, og = pl.pallas_call(
        kernel,
        out_shape=(shape((2, RY, 4 * HB), BF16), shape((2 * TB, 256), BF16)),
        in_specs=[hbm] * 4,
        out_specs=(hbm,) * 2,
        scratch_shapes=[
            bf(NY * TB, D), bf(NY * TB, D),
            bf(2, D, 2 * HB),
            bf(TB, 256), bf(TB, 256),
            bf(2, RY, 4 * HB),
            bf(NY * TB, 2 * HB),
            bf(2, 2 * HB, NY * TB),
            f4(2, TB, 2 * HB),
            f4(2, NZ, 2 * HB, DZ),
            bf(2, NZ, HB, DZ), bf(2, NZ, HB, DZ),
            bf(2, 7, HB, DZ), bf(2, 7, HB, DZ),
            bf(2, DZ, HB),
            bf(NY * TB, D),
            bf(2, 64, D), bf(2, 128, D), bf(2, 64, D),
            f4(NX, 128, FX),
            bf(2, 64, FX), bf(2, 128, FX), bf(3, 128, FX),
            bf(2, NY, 64, FX), bf(2, NY, 128, FX), bf(2, NY, 64, FX),
            f4(NY, 128, FX),
            bf(2, 64, FX), bf(2, 128, FX), bf(3, 128, FX),
            bf(2, TB, 256),
            pltpu.SemaphoreType.DMA((6,)),
            pltpu.SemaphoreType.DMA((SENDS,)),
            pltpu.SemaphoreType.DMA((RECVS,)),
        ],
        compiler_params=pltpu.CompilerParams(
            collective_id=0, has_side_effects=True, vmem_limit_bytes=60 * 1024 * 1024
        ),
    )(normed_input, cotangent, up_weight, down_weight.T)
    ig, ug, dg = pl.pallas_call(
        finisher,
        out_shape=(shape((2 * TB, 256), BF16), shape((RY, 4 * HB), F32), shape((RY, 4 * HB), F32)),
        in_specs=[hbm] * 2,
        out_specs=(hbm,) * 3,
        scratch_shapes=[
            bf(2, RY, 4 * HB), bf(2 * TB, 256), f4(2, RY, 4 * HB), pltpu.SemaphoreType.DMA((6,)),
        ],
    )(ow, og)
    return ig, ug, dg.T


def solution(mesh):
    return jax.shard_map(
        per_device, mesh=mesh,
        in_specs=(P("fs", "tp"), P("fs", "tp"), P("fs", "tp"), P("tp", "fs")),
        out_specs=(P("fs", "tp"), P("fs", "tp"), P("tp", "fs")),
        check_vma=False,
    )
```

time: 97.1 us -> 90.5 us (0.932)
  the two profiles are of different devices: /device:TPU:8 before, /device:TPU:1 now
where the time goes in v3:
time: 90.5 us; the launch traced here: 89.9 us
  Pallas kernels  89.3 us (99%)
    pallas_call x1, Pallas kernels, per_device(): pl.pallas_call(kernel, out_shape=(shape((2, RY, 4 * HB), BF16), shape((2...  87.4 us
    pallas_call x1, Pallas kernels, per_device(): pl.pallas_call(finisher, out_shape=(shape((2 * TB, 256), BF16), shape((RY...  1.85 us

profile of v3, /device:TPU:1, one launch (start us, length us, event | category | flops | bytes accessed | tf_op | source)
XLA Modules:
  0.0 89.9 jit_solution(8998391961877256445)
XLA Ops:
  0.6 87.4 %shard_map.67 = (bf16[2,64,1024]{2,1,0:T(8,128)(2,1)}, bf16[512,256]{1,0:T(8,128)(2,1)}) custom-call(bf16[512,256]{1,0:T(8,128)(2,1)} %x_in.1, bf16[512,256]{1,0:T(8,128)(2,1)} %c_in.1, bf16[64,1024]{1,0:T(8,128)(2,1)} %up_in.1, bf16[64,1024]{1,0:T(8,128)(2,1)} %bitcast.2), custom_call_target="tpu_custom_call" | custom-call | tf_op jit(solution)/shard_map/pallas_call | solution.py:475
  88.1 1.9 %shard_map.68 = (bf16[512,256]{1,0:T(8,128)(2,1)}, f32[64,1024]{1,0:T(8,128)}, f32[64,1024]{1,0:T(8,128)}) custom-call(bf16[2,64,1024]{2,1,0:T(8,128)(2,1)} %get-tuple-element.8.ow, bf16[512,256]{1,0:T(8,128)(2,1)} %get-tuple-element.9.og), custom_call_target="tpu_custom_call" | custom-call | tf_op jit(solution)/shard_map/pallas_call | solution.py:508

commit v4 on v3

--- a/solution.py
+++ b/solution.py
@@ -15,8 +15,9 @@
 DZ = 256
 RY = 64
 HALF = TB // 2
-SPLIT = (128, 112)
-SENDS, RECVS = 10, 72
+CUT = 112
+MID = (96, 160)
+SENDS, RECVS = 6, 61
 MESH = pl.DeviceIdType.MESH
 BF16, F32 = jnp.bfloat16, jnp.float32
 
@@ -31,7 +32,7 @@
 
 def kernel(
     x_in, c_in, up_in, dn_in, ow, og,
-    xb, cb, w, xs, cs, uv, pg, tr, acc, gt, gs, pb, rz, sz, fs_s, g,
+    xb, cb, w, xs, cs, uv, pg, tr, acc, gp, gt, gs, pb, rz, sz, fs_s, g,
     ra, rb, sb, q1, rc, rd, sd, re, rf, sf, q2, rg, rh, sh, fp,
     lsem, ssem, rsem,
 ):
@@ -114,6 +115,10 @@
     loads[1].wait()
     xop = send(xs, xb.at[0:TB, mine], PC)
     loads[2].wait()
+    loads[3].wait()
+    x_x = Batch()
+    for way in (XR, XL):
+        x_x.send(xb.at[0:TB, mine], xb.at[0:TB, mine], way)
     wops = Batch()
     for ay, where in ((y2, Y2), (yr, YR), (yl, YL)):
         for u in range(2):
@@ -130,24 +135,23 @@
         ref = blk(buf, ME, ax)
         return send(ref, blk(buf, L, ax), YR).send(ref, blk(buf, R, ax), YL)
 
-    def pass_x(buf, slot, batch, out=None):
+    def pass_x(buf, slot, batch):
         batch.wait()
-        cut = SPLIT[0]
-        a, b = blk(buf, slot, xl, 0, cut), blk(buf, slot, xr, cut)
-        return (out or Batch()).send(a, a, XR).send(b, b, XL)
-
-    def pass_y(buf, ax, batch, out=None):
+        a, b = blk(buf, slot, xl, 0, HALF), blk(buf, slot, xr, HALF)
+        return send(a, a, XR).send(b, b, XL)
+
+    def pass_y(buf, ax, batch, out=None, lo=CUT, hi=CUT):
         batch.wait()
-        cut = SPLIT[1]
         out = out or Batch()
-        out.send(blk(buf, L, ax, 0, cut), blk(buf, OPP, ax, 0, cut), YR)
-        return out.send(blk(buf, R, ax, cut), blk(buf, OPP, ax, cut), YL)
-
-    loads[3].wait()
+        out.send(blk(buf, L, ax, 0, lo), blk(buf, OPP, ax, 0, lo), YR)
+        return out.send(blk(buf, R, ax, hi), blk(buf, OPP, ax, hi), YL)
+
     cop.wait()
     c_y = over_y(cb, x)
+    there = pl.ds(pl.multiple_of(x * FX + o * 256, 256), 256)
     xop.wait()
-    x_x = over_x(xb, ME, x)
+    for way in (XR, XL):
+        x_x.send(xb.at[0:TB, there], xb.at[0:TB, there], way)
     x_y = {"me": over_y(xb, x)}
     c_x = {"me": over_x(cb, ME, x)}
 
@@ -197,12 +201,12 @@
     fx.wait()
     x_y["2"] = over_y(xb, x2)
     warrive(3)
-    fxy = pass_y(xb, x, x_y["me"])
+    fxym = pass_y(xb, x, x_y["me"])
     fc.wait()
     warrive(4)
     warrive(5)
     fcx["l"] = pass_x(cb, L, c_x["l"])
-    pass_y(xb, xl, x_y["l"], fxy)
+    fxy = pass_y(xb, xl, x_y["l"], None, *MID)
     warrive(6)
     fcx["me"].wait()
     wpc.wait()
@@ -237,7 +241,7 @@
     c2 = send(lo, lo, XR).send(hi, hi, XL)
     c3 = send(hi, hi, XR).send(lo, lo, XL)
     partial(ME, L)
-    pass_y(xb, xr, x_y["r"], fxy)
+    pass_y(xb, xr, x_y["r"], fxy, *MID)
     fxy2 = pass_y(xb, x2, x_y["2"])
     fcx["l"].wait()
     forward(L)
@@ -245,6 +249,9 @@
     forward(R)
     fcx["2"] = pass_x(cb, OPP, c2)
     partial(L, OPP)
+    fxym.wait()
+    mid = blk(xb, OPP, x, *MID)
+    fmid = send(mid, mid, XR).send(mid, mid, XL)
 
     def part(slot, r, n, lane=slice(None)):
         return g.at[slot * TB + r:slot * TB + r + n, lane]
@@ -276,26 +283,6 @@
     h2early = first_x((ME, L, R))
     for slot in (ME, L, R):
         next_x(slot)
-
-    for u, buf in ((0, xb), (1, cb)):
-        @pl.loop(0, NZ, unroll=2)
-        def _(k):
-            gt[u, k] = nn(tr[u, :, 0:3 * TB], buf[0:3 * TB, cols(k, DZ)])
-
-    orow = slice(OPP * TB, OPP * TB + TB)
-    c3.wait()
-    fcx["2"].wait()
-    for h in range(2):
-        s = slice(h * HB, (h + 1) * HB)
-        acc[1, :, s] = nn(cb[orow], w[1, :, s])
-    fxy.wait()
-    for n, ax in enumerate((x, xl, xr)):
-        lane = cols(ax, FX)
-        term = nn(xb[orow, lane], w[0, lane, :])
-        acc[0] = term if n == 0 else acc[0] + term
-    fxy2.wait()
-    pre = acc[0] + nn(xb[orow, far], w[0, far, :])
-    finish(OPP, slice(0, 2 * HB), pre, acc[1])
 
     down = ([(0, 4), (1, 3), (0, 3), (1, 2), (0, 2), (1, 1), (0, 1)],
             [(1, 4), (0, 3), (1, 3), (0, 2), (1, 2), (0, 1), (1, 1)])
@@ -307,21 +294,63 @@
     todo += [(0, 0), (1, 0)]
     wsum = []
 
-    def chunks(i):
+    def term(n, rows, lo, hi):
+        u, k = todo[n]
+        return nn(tr[u, rows, lo * TB:hi * TB], (xb, cb)[u][lo * TB:hi * TB, cols(step(z, k, NZ), DZ)])
+
+    def early(*which):
+        for n in which:
+            gp[n] = term(n, slice(None), 0, 3)
+
+    def give(batch, n, value):
+        u, k = todo[n]
+        az = step(z, k, NZ)
+        gs[u, az] = value.astype(BF16)
+        batch.send(gs.at[u, az], pb.at[u, az], PC)
+
+    def keep(n, value):
+        u, k = todo[n]
+        gt[u, step(z, k, NZ)] = value
+
+    def chunks(i, split=False):
         batch = Batch()
-        for u, k in todo[2 * i:2 * i + 2]:
-            az = step(z, k, NZ)
-            value = gt[u, az] + nn(tr[u, :, 3 * TB:], (xb, cb)[u][orow, cols(az, DZ)])
-            gs[u, az] = value[HB:].astype(BF16)
-            batch.send(gs.at[u, az], pb.at[u, az], PC)
-            gt[u, az, 0:HB] = value[:HB]
+        pair = (2 * i, 2 * i + 1)
+        if split:
+            for n in pair:
+                give(batch, n, gp[n, HB:] + term(n, slice(HB, 2 * HB), 3, 4))
+            for n in pair:
+                keep(n, gp[n, :HB] + term(n, slice(0, HB), 3, 4))
+        else:
+            for n in pair:
+                value = gp[n] + term(n, slice(None), 3, 4)
+                give(batch, n, value[HB:])
+                keep(n, value[:HB])
         wsum.append(batch)
+
+    early(*range(14))
+
+    orow = slice(OPP * TB, OPP * TB + TB)
+    c3.wait()
+    fcx["2"].wait()
+    for h in range(2):
+        s = slice(h * HB, (h + 1) * HB)
+        acc[1, :, s] = nn(cb[orow], w[1, :, s])
+    early(14, 15)
+    fxy.wait()
+    fmid.wait()
+    for n, ax in enumerate((x, xl, xr)):
+        lane = cols(ax, FX)
+        more = nn(xb[orow, lane], w[0, lane, :])
+        acc[0] = more if n == 0 else acc[0] + more
+    fxy2.wait()
+    pre = acc[0] + nn(xb[orow, far], w[0, far, :])
+    finish(OPP, slice(0, 2 * HB), pre, acc[1])
 
     gz = []
 
     def total(u, k):
         az = step(z, k, NZ)
-        return gt[u, az, 0:HB] + pb[u, az].astype(F32)
+        return gt[u, az] + pb[u, az].astype(F32)
 
     def gsend(i):
         wsum[i].wait()
@@ -334,10 +363,17 @@
             if i >= 2:
                 value = value + rz[way, i - 2].astype(F32)
             sz[way, i] = value.astype(BF16)
-            batch.send(sz.at[way, i], rz.at[way, i], (ZR, ZL)[way])
+            if i < 6:
+                batch.send(sz.at[way, i], rz.at[way, i], (ZR, ZL)[way])
         gz.append(batch)
-
-    chunks(0)
+        if i == 6:
+            for rows in (slice(0, 128), slice(128, 256)):
+                batch = Batch()
+                for way in range(2):
+                    batch.send(sz.at[way, i, rows], rz.at[way, i, rows], (ZR, ZL)[way])
+                gz.append(batch)
+
+    chunks(0, split=True)
     chunks(1)
     gsend(0)
     partial(OPP, OPP + 1)
@@ -354,7 +390,6 @@
     chunks(2)
     gsend(2)
     chunks(3)
-    chunks(4)
     def next_y(n, r):
         h1[n].wait()
         sb[0, r:r + 32] = (part(R, r, 32)[...].astype(F32) + ra[0, r:r + 32].astype(F32)).astype(BF16)
@@ -367,11 +402,9 @@
     h2[OPP].wait()
     last_x(OPP)
     next_y(1, 32)
+    chunks(4)
+    gsend(4)
     chunks(5)
-    chunks(6)
-    gsend(4)
-    chunks(7)
-    gsend(5)
 
     h2b.wait()
     here = cols(x, FX)
@@ -385,6 +418,7 @@
     v2b = Batch()
     v2b.send(sh.at[1, 64:128, :], rh.at[0, 64:128, :], YR)
     v2b.send(sh.at[2, 0:64, :], rh.at[1, 0:64, :], YL)
+    gsend(5)
     h1b.wait()
     for k in range(NX):
         s = slice(k * FX, (k + 1) * FX)
@@ -396,12 +430,14 @@
     v1b = Batch()
     v1b.send(sd.at[1, 64:128, :], rd.at[0, 64:128, :], XR)
     v1b.send(sd.at[2, 0:64, :], rd.at[1, 0:64, :], XL)
-    gsend(6)
+    chunks(6)
+    chunks(7)
     v2.wait()
     sh[1, 0:64] = (q2[R, 0:64, :] + rg[0].astype(F32)).astype(BF16)
     v2b.send(sh.at[1, 0:64, :], rh.at[0, 0:64, :], YR)
     sh[2, 64:128] = (q2[L, 64:128, :] + rg[1].astype(F32)).astype(BF16)
     v2b.send(sh.at[2, 64:128, :], rh.at[1, 64:128, :], YL)
+    gsend(6)
     v1.wait()
     sd[1, 0:64] = (q1[xr, 0:64, :] + rc[0].astype(F32)).astype(BF16)
     v1b.send(sd.at[1, 0:64, :], rd.at[0, 0:64, :], XR)
@@ -423,23 +459,27 @@
         ends.send(fp.at[0, r:r + 128], og.at[row, :], PC)
         store(fp.at[1, r:r + 128], og.at[row, :])
 
+    scale = 1.0 / 128.0
+    ops = Batch()
+    wsum[7].wait()
+    gz[5].wait()
+    for half in range(2):
+        gz[7 + half].wait()
+        rows = slice(half * 128, half * 128 + 128)
+        lane = pl.ds(pl.multiple_of(y * HB + half * 128, 128), 128)
+        for u in range(2):
+            value = gt[u, z, rows] + pb[u, z, rows].astype(F32)
+            value = value + rz[0, 6 - u, rows].astype(F32) + rz[1, 5 + u, rows].astype(F32)
+            fs_s[u, half] = (value * scale).T.astype(BF16)
+            for ay, where in ((y2, Y2), (yr, YR), (yl, YL)):
+                ops.send(fs_s.at[u, half, cols(ay, RY), :], ow.at[u, :, lane], where, small=True)
+            store(fs_s.at[u, half, cols(y, RY), :], ow.at[u, :, lane])
+
     v1b.wait()
     finish_rows(0, q1[x] + rd[0].astype(F32) + rd[1].astype(F32), 0)
     v2b.wait()
     finish_rows(128, q2[ME] + rh[0].astype(F32) + rh[1].astype(F32), 1)
 
-    scale = 1.0 / 128.0
-    ops = Batch()
-    wsum[7].wait()
-    gz[5].wait()
-    gz[6].wait()
-    for u in range(2):
-        value = total(u, 0) + rz[0, 6 - u].astype(F32) + rz[1, 5 + u].astype(F32)
-        fs_s[u] = (value * scale).T.astype(BF16)
-        there = cols(y, HB)
-        for ay, where in ((y2, Y2), (yr, YR), (yl, YL)):
-            ops.send(fs_s.at[u, cols(ay, RY), :], ow.at[u, :, there], where, small=True)
-        store(fs_s.at[u, cols(y, RY), :], ow.at[u, :, there])
     ops.wait()
     ends.wait()
     ref = span(stored[0])
@@ -485,10 +525,11 @@
             bf(NY * TB, 2 * HB),
             bf(2, 2 * HB, NY * TB),
             f4(2, TB, 2 * HB),
-            f4(2, NZ, 2 * HB, DZ),
+            f4(2 * NZ, 2 * HB, DZ),
+            f4(2, NZ, HB, DZ),
             bf(2, NZ, HB, DZ), bf(2, NZ, HB, DZ),
             bf(2, 7, HB, DZ), bf(2, 7, HB, DZ),
-            bf(2, DZ, HB),
+            bf(2, 2, DZ, 128),
             bf(NY * TB, D),
             bf(2, 64, D), bf(2, 128, D), bf(2, 64, D),
             f4(NX, 128, FX),

time: 90.5 us -> 88.8 us (0.981)
  Pallas kernels: 89.3 us -> 88.1 us
    pallas_call x1, Pallas kernels: 87.4 us -> 86.2 us  [per_device(): pl.pallas_call(kernel, out_shape=(shape((2, RY, 4 * HB), BF16), shape((2...]
where the time goes in v4:
time: 88.8 us; the launch traced here: 88.7 us
  Pallas kernels  88.1 us (99%)
    pallas_call x1, Pallas kernels, per_device(): pl.pallas_call(kernel, out_shape=(shape((2, RY, 4 * HB), BF16), shape((2...  86.2 us
    pallas_call x1, Pallas kernels, per_device(): pl.pallas_call(finisher, out_shape=(shape((2 * TB, 256), BF16), shape((RY...  1.85 us

profile of v4, /device:TPU:1, one launch (start us, length us, event | category | flops | bytes accessed | tf_op | source)
XLA Modules:
  0.0 88.7 jit_solution(15414190035344686235)
XLA Ops:
  0.6 86.2 %shard_map.67 = (bf16[2,64,1024]{2,1,0:T(8,128)(2,1)}, bf16[512,256]{1,0:T(8,128)(2,1)}) custom-call(bf16[512,256]{1,0:T(8,128)(2,1)} %x_in.1, bf16[512,256]{1,0:T(8,128)(2,1)} %c_in.1, bf16[64,1024]{1,0:T(8,128)(2,1)} %up_in.1, bf16[64,1024]{1,0:T(8,128)(2,1)} %bitcast.2), custom_call_target="tpu_custom_call" | custom-call | tf_op jit(solution)/shard_map/pallas_call | solution.py:515
  86.9 1.9 %shard_map.68 = (bf16[512,256]{1,0:T(8,128)(2,1)}, f32[64,1024]{1,0:T(8,128)}, f32[64,1024]{1,0:T(8,128)}) custom-call(bf16[2,64,1024]{2,1,0:T(8,128)(2,1)} %get-tuple-element.8.ow, bf16[512,256]{1,0:T(8,128)(2,1)} %get-tuple-element.9.og), custom_call_target="tpu_custom_call" | custom-call | tf_op jit(solution)/shard_map/pallas_call | solution.py:549

commit v5 on v4

--- a/solution.py
+++ b/solution.py
@@ -17,7 +17,7 @@
 HALF = TB // 2
 CUT = 112
 MID = (96, 160)
-SENDS, RECVS = 6, 61
+SENDS, RECVS = 6, 66
 MESH = pl.DeviceIdType.MESH
 BF16, F32 = jnp.bfloat16, jnp.float32
 
@@ -48,6 +48,8 @@
     YR, YL, Y2 = at(x, yr, z, c), at(x, yl, z, c), at(x, y2, z, c)
     ZR, ZL = at(x, y, step(z, 1, NZ), c), at(x, y, step(z, -1, NZ), c)
     PC = at(x, y, z, o)
+    mate = y + 1 - 2 * lax.rem(y, 2)
+    MATE, ACROSS = at(x, mate, z, c), at(x, step(mate, 2, NY), z, c)
     ME, L, R, OPP = range(4)
 
     arrivals = iter(range(RECVS))
@@ -312,19 +314,22 @@
         u, k = todo[n]
         gt[u, step(z, k, NZ)] = value
 
-    def chunks(i, split=False):
+    def give_pair(i):
         batch = Batch()
-        pair = (2 * i, 2 * i + 1)
-        if split:
-            for n in pair:
-                give(batch, n, gp[n, HB:] + term(n, slice(HB, 2 * HB), 3, 4))
-            for n in pair:
-                keep(n, gp[n, :HB] + term(n, slice(0, HB), 3, 4))
-        else:
-            for n in pair:
-                value = gp[n] + term(n, slice(None), 3, 4)
-                give(batch, n, value[HB:])
-                keep(n, value[:HB])
+        for n in (2 * i, 2 * i + 1):
+            give(batch, n, gp[n, HB:] + term(n, slice(HB, 2 * HB), 3, 4))
+        wsum.append(batch)
+
+    def keep_pair(i):
+        for n in (2 * i, 2 * i + 1):
+            keep(n, gp[n, :HB] + term(n, slice(0, HB), 3, 4))
+
+    def chunks(i):
+        batch = Batch()
+        for n in (2 * i, 2 * i + 1):
+            value = gp[n] + term(n, slice(None), 3, 4)
+            give(batch, n, value[HB:])
+            keep(n, value[:HB])
         wsum.append(batch)
 
     early(*range(14))
@@ -343,38 +348,42 @@
         more = nn(xb[orow, lane], w[0, lane, :])
         acc[0] = more if n == 0 else acc[0] + more
     fxy2.wait()
-    pre = acc[0] + nn(xb[orow, far], w[0, far, :])
-    finish(OPP, slice(0, 2 * HB), pre, acc[1])
+    for h in (1, 0):
+        s = slice(h * HB, (h + 1) * HB)
+        finish(OPP, s, acc[0, :, s] + nn(xb[orow, far], w[0, far, s]), acc[1, :, s])
+        if h == 1:
+            give_pair(0)
+            give_pair(1)
 
     gz = []
 
-    def total(u, k):
+    away = 1 - lax.div(y, 2)
+    sides = (cols(away, DZ // 2), cols(1 - away, DZ // 2))
+
+    def total(u, k, lane):
         az = step(z, k, NZ)
-        return gt[u, az] + pb[u, az].astype(F32)
+        return gt[u, az, :, lane] + pb[u, az, :, lane].astype(F32)
 
     def gsend(i):
         wsum[i].wait()
-        if i >= 2:
-            gz[i - 2].wait()
-        batch = Batch()
-        for way in range(2):
-            u, k = down[way][i]
-            value = total(u, k if way == 0 else -k)
+        halves = []
+        for half, lane in enumerate(sides):
             if i >= 2:
-                value = value + rz[way, i - 2].astype(F32)
-            sz[way, i] = value.astype(BF16)
-            if i < 6:
-                batch.send(sz.at[way, i], rz.at[way, i], (ZR, ZL)[way])
-        gz.append(batch)
-        if i == 6:
-            for rows in (slice(0, 128), slice(128, 256)):
-                batch = Batch()
-                for way in range(2):
-                    batch.send(sz.at[way, i, rows], rz.at[way, i, rows], (ZR, ZL)[way])
-                gz.append(batch)
-
-    chunks(0, split=True)
-    chunks(1)
+                gz[i - 2][half].wait()
+            batch = Batch()
+            for way in range(2):
+                u, k = down[way][i]
+                value = total(u, k if way == 0 else -k, lane)
+                if i >= 2:
+                    value = value + rz[way, i - 2, :, lane].astype(F32)
+                sz[way, i, :, lane] = value.astype(BF16)
+                ref = (way, i, slice(None), lane)
+                batch.send(sz.at[ref], rz.at[ref], (ZR, ZL)[way])
+            halves.append(batch)
+        gz.append(halves)
+
+    keep_pair(0)
+    keep_pair(1)
     gsend(0)
     partial(OPP, OPP + 1)
     h1 = []
@@ -405,6 +414,7 @@
     chunks(4)
     gsend(4)
     chunks(5)
+    gsend(5)
 
     h2b.wait()
     here = cols(x, FX)
@@ -418,7 +428,8 @@
     v2b = Batch()
     v2b.send(sh.at[1, 64:128, :], rh.at[0, 64:128, :], YR)
     v2b.send(sh.at[2, 0:64, :], rh.at[1, 0:64, :], YL)
-    gsend(5)
+    chunks(6)
+    chunks(7)
     h1b.wait()
     for k in range(NX):
         s = slice(k * FX, (k + 1) * FX)
@@ -430,14 +441,12 @@
     v1b = Batch()
     v1b.send(sd.at[1, 64:128, :], rd.at[0, 64:128, :], XR)
     v1b.send(sd.at[2, 0:64, :], rd.at[1, 0:64, :], XL)
-    chunks(6)
-    chunks(7)
+    gsend(6)
     v2.wait()
     sh[1, 0:64] = (q2[R, 0:64, :] + rg[0].astype(F32)).astype(BF16)
     v2b.send(sh.at[1, 0:64, :], rh.at[0, 0:64, :], YR)
     sh[2, 64:128] = (q2[L, 64:128, :] + rg[1].astype(F32)).astype(BF16)
     v2b.send(sh.at[2, 64:128, :], rh.at[1, 64:128, :], YL)
-    gsend(6)
     v1.wait()
     sd[1, 0:64] = (q1[xr, 0:64, :] + rc[0].astype(F32)).astype(BF16)
     v1b.send(sd.at[1, 0:64, :], rd.at[0, 0:64, :], XR)
@@ -445,35 +454,33 @@
     v1b.send(sd.at[2, 64:128, :], rd.at[1, 64:128, :], XL)
     own, other = cols(c, 256), cols(o, 256)
     ends = Batch()
-    stored = [0]
-
-    def store(src, dst):
-        pltpu.make_async_copy(src, dst, lsem.at[5]).start()
-        stored[0] += size(src)
-
     def finish_rows(r, value, n):
         q1[n] = value
-        fp[0, r:r + 128] = q1[n, :, other].astype(BF16)
-        fp[1, r:r + 128] = q1[n, :, own].astype(BF16)
+        fp[r:r + 128] = q1[n, :, other].astype(BF16)
         row = pl.ds(pl.multiple_of(c * TB + r, 128), 128)
-        ends.send(fp.at[0, r:r + 128], og.at[row, :], PC)
-        store(fp.at[1, r:r + 128], og.at[row, :])
+        ends.send(fp.at[r:r + 128], og.at[row, :], PC)
+        og[row, :] = q1[n, :, own].astype(BF16)
 
     scale = 1.0 / 128.0
     ops = Batch()
     wsum[7].wait()
-    gz[5].wait()
-    for half in range(2):
-        gz[7 + half].wait()
-        rows = slice(half * 128, half * 128 + 128)
-        lane = pl.ds(pl.multiple_of(y * HB + half * 128, 128), 128)
+    there = cols(y, HB)
+    for half, lane in enumerate(sides):
+        gz[5][half].wait()
+        gz[6][half].wait()
         for u in range(2):
-            value = gt[u, z, rows] + pb[u, z, rows].astype(F32)
-            value = value + rz[0, 6 - u, rows].astype(F32) + rz[1, 5 + u, rows].astype(F32)
+            value = total(u, 0, lane)
+            value = value + rz[0, 6 - u, :, lane].astype(F32) + rz[1, 5 + u, :, lane].astype(F32)
             fs_s[u, half] = (value * scale).T.astype(BF16)
-            for ay, where in ((y2, Y2), (yr, YR), (yl, YL)):
-                ops.send(fs_s.at[u, half, cols(ay, RY), :], ow.at[u, :, lane], where, small=True)
-            store(fs_s.at[u, half, cols(y, RY), :], ow.at[u, :, lane])
+            if half == 0:
+                odd = lax.rem(y, 2)
+                near = 1 - odd
+                ops.send(fs_s.at[u, 0, cols(odd, RY), :], ow.at[u, :, there], Y2, small=True)
+                ops.send(fs_s.at[u, 0, cols(near, RY), :], ow.at[u, :, there], ACROSS, small=True)
+            else:
+                odd = lax.rem(y, 2)
+                ops.send(fs_s.at[u, 1, cols(1 - odd, RY), :], ow.at[u, :, there], MATE, small=True)
+                ow[u, :, there] = fs_s[u, 1, cols(odd, RY), :]
 
     v1b.wait()
     finish_rows(0, q1[x] + rd[0].astype(F32) + rd[1].astype(F32), 0)
@@ -482,27 +489,18 @@
 
     ops.wait()
     ends.wait()
-    ref = span(stored[0])
-    pltpu.make_async_copy(ref, ref, lsem.at[5]).wait()
     for k, (n, _) in enumerate(groups):
         ref = span(n)
         pltpu.make_async_copy(ref, ref, ssem.at[k]).wait()
 
 
-def finisher(ow, og, ig_out, ug_out, dg_out, wv, gv, fv, sem):
-    loads = [pltpu.make_async_copy(ow.at[u], wv.at[u], sem.at[u]) for u in range(2)]
-    loads.append(pltpu.make_async_copy(og, gv, sem.at[2]))
-    for copy in loads:
-        copy.start()
-    stores = []
+def finisher(ow, og, ig_out, ug_out, dg_out, fv, sem):
+    stores = [pltpu.make_async_copy(og, ig_out, sem.at[0])]
+    stores[0].start()
     for u, out in ((0, ug_out), (1, dg_out)):
-        loads[u].wait()
-        fv[u] = wv[u].astype(F32)
-        stores.append(pltpu.make_async_copy(fv.at[u], out, sem.at[3 + u]))
+        fv[u] = ow[u].astype(F32)
+        stores.append(pltpu.make_async_copy(fv.at[u], out, sem.at[1 + u]))
         stores[-1].start()
-    loads[2].wait()
-    stores.append(pltpu.make_async_copy(gv, ig_out, sem.at[5]))
-    stores[-1].start()
     for copy in stores:
         copy.wait()
 
@@ -511,12 +509,13 @@
     bf = lambda *s: pltpu.VMEM(s, BF16)
     f4 = lambda *s: pltpu.VMEM(s, F32)
     hbm = pl.BlockSpec(memory_space=pl.ANY)
+    vmem = pl.BlockSpec(memory_space=pltpu.VMEM)
     shape = jax.ShapeDtypeStruct
     ow, og = pl.pallas_call(
         kernel,
-        out_shape=(shape((2, RY, 4 * HB), BF16), shape((2 * TB, 256), BF16)),
+        out_shape=(bf(2, RY, 4 * HB), bf(2 * TB, 256)),
         in_specs=[hbm] * 4,
-        out_specs=(hbm,) * 2,
+        out_specs=(vmem,) * 2,
         scratch_shapes=[
             bf(NY * TB, D), bf(NY * TB, D),
             bf(2, D, 2 * HB),
@@ -529,7 +528,7 @@
             f4(2, NZ, HB, DZ),
             bf(2, NZ, HB, DZ), bf(2, NZ, HB, DZ),
             bf(2, 7, HB, DZ), bf(2, 7, HB, DZ),
-            bf(2, 2, DZ, 128),
+            bf(2, 2, DZ // 2, HB),
             bf(NY * TB, D),
             bf(2, 64, D), bf(2, 128, D), bf(2, 64, D),
             f4(NX, 128, FX),
@@ -537,8 +536,8 @@
             bf(2, NY, 64, FX), bf(2, NY, 128, FX), bf(2, NY, 64, FX),
             f4(NY, 128, FX),
             bf(2, 64, FX), bf(2, 128, FX), bf(3, 128, FX),
-            bf(2, TB, 256),
-            pltpu.SemaphoreType.DMA((6,)),
+            bf(TB, 256),
+            pltpu.SemaphoreType.DMA((5,)),
             pltpu.SemaphoreType.DMA((SENDS,)),
             pltpu.SemaphoreType.DMA((RECVS,)),
         ],
@@ -549,12 +548,10 @@
     ig, ug, dg = pl.pallas_call(
         finisher,
         out_shape=(shape((2 * TB, 256), BF16), shape((RY, 4 * HB), F32), shape((RY, 4 * HB), F32)),
-        in_specs=[hbm] * 2,
+        in_specs=[vmem] * 2,
         out_specs=(hbm,) * 3,
-        scratch_shapes=[
-            bf(2, RY, 4 * HB), bf(2 * TB, 256), f4(2, RY, 4 * HB), pltpu.SemaphoreType.DMA((6,)),
-        ],
-    )(ow, og)
+        scratch_shapes=[f4(2, RY, 4 * HB), pltpu.SemaphoreType.DMA((3,))],
+    )(*(pltpu.with_memory_space_constraint(a, pltpu.VMEM) for a in (ow, og)))
     return ig, ug, dg.T
 
 

time: 88.8 us -> 88 us (level)
  Pallas kernels: 88.1 us -> 87.1 us
    pallas_call x1, Pallas kernels: 1.85 us -> 0.9 us  [per_device(): pl.pallas_call(finisher, out_shape=(shape((2 * TB, 256), BF16), shape((RY...]
where the time goes in v5:
time: 88 us; the launch traced here: 87.9 us
  Pallas kernels  87.1 us (99%)
    pallas_call x1, Pallas kernels, per_device(): pl.pallas_call(kernel, out_shape=(bf(2, RY, 4 * HB), bf(2 * TB, 256)), in...  86.2 us

profile of v5, /device:TPU:1, one launch (start us, length us, event | category | flops | bytes accessed | tf_op | source)
XLA Modules:
  0.0 87.9 jit_solution(15936018039954299388)
XLA Ops:
  0.6 86.2 %shard_map.67 = (bf16[2,64,1024]{2,1,0:T(8,128)(2,1)S(1)}, bf16[512,256]{1,0:T(8,128)(2,1)S(1)}) custom-call(bf16[512,256]{1,0:T(8,128)(2,1)} %x_in.1, bf16[512,256]{1,0:T(8,128)(2,1)} %c_in.1, bf16[64,1024]{1,0:T(8,128)(2,1)} %up_in.1, bf16[64,1024]{1,0:T(8,128)(2,1)} %bitcast.2), custom_call_target="tpu_custom_call" | custom-call | tf_op jit(solution)/shard_map/pallas_call | solution.py:514
  86.8 0.9 %shard_map.68 = (bf16[512,256]{1,0:T(8,128)(2,1)}, f32[64,1024]{1,0:T(8,128)}, f32[64,1024]{1,0:T(8,128)}) custom-call(bf16[2,64,1024]{2,1,0:T(8,128)(2,1)S(1)} %get-tuple-element.8.ow, bf16[512,256]{1,0:T(8,128)(2,1)S(1)} %get-tuple-element.9.og), custom_call_target="tpu_custom_call" | custom-call | tf_op jit(solution)/shard_map/pallas_call | solution.py:548

commit v6 on v5

--- a/solution.py
+++ b/solution.py
@@ -17,7 +17,7 @@
 HALF = TB // 2
 CUT = 112
 MID = (96, 160)
-SENDS, RECVS = 6, 66
+SENDS, RECVS = 6, 67
 MESH = pl.DeviceIdType.MESH
 BF16, F32 = jnp.bfloat16, jnp.float32
 
@@ -230,9 +230,9 @@
         tr[1, s, rows] = (rect * rect).T.astype(BF16)
 
     def partial(lo, hi):
-        rows = slice(lo * TB, hi * TB)
-
-        @pl.loop(0, NZ, unroll=2)
+        rows = slice(lo, hi)
+
+        @pl.loop(0, NZ, unroll=4)
         def _(k):
             lane = cols(k, DZ)
             g[rows, lane] = nt(pg[rows, :], w[0, lane, :]).astype(BF16)
@@ -242,7 +242,7 @@
     lo, hi = blk(cb, OPP, x, 0, HALF), blk(cb, OPP, x, HALF)
     c2 = send(lo, lo, XR).send(hi, hi, XL)
     c3 = send(hi, hi, XR).send(lo, lo, XL)
-    partial(ME, L)
+    partial(ME * TB, L * TB)
     pass_y(xb, xr, x_y["r"], fxy, *MID)
     fxy2 = pass_y(xb, x2, x_y["2"])
     fcx["l"].wait()
@@ -250,7 +250,7 @@
     fcx["r"].wait()
     forward(R)
     fcx["2"] = pass_x(cb, OPP, c2)
-    partial(L, OPP)
+    partial(L * TB, OPP * TB)
     fxym.wait()
     mid = blk(xb, OPP, x, *MID)
     fmid = send(mid, mid, XR).send(mid, mid, XL)
@@ -353,43 +353,47 @@
         finish(OPP, s, acc[0, :, s] + nn(xb[orow, far], w[0, far, s]), acc[1, :, s])
         if h == 1:
             give_pair(0)
-            give_pair(1)
 
     gz = []
 
     away = 1 - lax.div(y, 2)
     sides = (cols(away, DZ // 2), cols(1 - away, DZ // 2))
 
-    def total(u, k, lane):
+    WHOLE, TOP, LOW = slice(None), slice(0, HB // 2), slice(HB // 2, HB)
+
+    def total(u, k, lane, rows=WHOLE):
         az = step(z, k, NZ)
-        return gt[u, az, :, lane] + pb[u, az, :, lane].astype(F32)
-
-    def gsend(i):
-        wsum[i].wait()
-        halves = []
-        for half, lane in enumerate(sides):
+        return gt[u, az, rows, lane] + pb[u, az, rows, lane].astype(F32)
+
+    def gsend(i, halves=(0, 1)):
+        if 0 in halves:
+            wsum[i].wait()
+            gz.append([])
+        for half in halves:
+            lane = sides[half]
             if i >= 2:
                 gz[i - 2][half].wait()
-            batch = Batch()
-            for way in range(2):
-                u, k = down[way][i]
-                value = total(u, k if way == 0 else -k, lane)
-                if i >= 2:
-                    value = value + rz[way, i - 2, :, lane].astype(F32)
-                sz[way, i, :, lane] = value.astype(BF16)
-                ref = (way, i, slice(None), lane)
-                batch.send(sz.at[ref], rz.at[ref], (ZR, ZL)[way])
-            halves.append(batch)
-        gz.append(halves)
+            for rows in (TOP, LOW) if (i, half) == (6, 1) else (WHOLE,):
+                batch = Batch()
+                for way in range(2):
+                    u, k = down[way][i]
+                    value = total(u, k if way == 0 else -k, lane, rows)
+                    if i >= 2:
+                        value = value + rz[way, i - 2, rows, lane].astype(F32)
+                    sz[way, i, rows, lane] = value.astype(BF16)
+                    ref = (way, i, rows, lane)
+                    batch.send(sz.at[ref], rz.at[ref], (ZR, ZL)[way])
+                gz[i].append(batch)
 
     keep_pair(0)
-    keep_pair(1)
-    gsend(0)
-    partial(OPP, OPP + 1)
+    partial(OPP * TB, OPP * TB + HALF)
     h1 = []
     for r in (0, 32):
         h1.append(send(part(OPP, r, 32), ra.at[0, r:r + 32], YR)
                   .send(part(OPP, 64 + r, 32), ra.at[1, r:r + 32], YL))
+    gsend(0)
+    chunks(1)
+    partial(OPP * TB + HALF, OPP * TB + TB)
     first_x((OPP,))
     next_x(OPP)
     gsend(1)
@@ -414,7 +418,8 @@
     chunks(4)
     gsend(4)
     chunks(5)
-    gsend(5)
+    chunks(6)
+    gsend(5, (0,))
 
     h2b.wait()
     here = cols(x, FX)
@@ -428,7 +433,6 @@
     v2b = Batch()
     v2b.send(sh.at[1, 64:128, :], rh.at[0, 64:128, :], YR)
     v2b.send(sh.at[2, 0:64, :], rh.at[1, 0:64, :], YL)
-    chunks(6)
     chunks(7)
     h1b.wait()
     for k in range(NX):
@@ -441,7 +445,9 @@
     v1b = Batch()
     v1b.send(sd.at[1, 64:128, :], rd.at[0, 64:128, :], XR)
     v1b.send(sd.at[2, 0:64, :], rd.at[1, 0:64, :], XL)
-    gsend(6)
+    gsend(6, (0,))
+    gsend(5, (1,))
+    gsend(6, (1,))
     v2.wait()
     sh[1, 0:64] = (q2[R, 0:64, :] + rg[0].astype(F32)).astype(BF16)
     v2b.send(sh.at[1, 0:64, :], rh.at[0, 0:64, :], YR)
@@ -465,22 +471,29 @@
     ops = Batch()
     wsum[7].wait()
     there = cols(y, HB)
-    for half, lane in enumerate(sides):
-        gz[5][half].wait()
-        gz[6][half].wait()
+    odd = lax.rem(y, 2)
+    near = 1 - odd
+
+    def zlast(u, lane, rows=WHOLE):
+        value = total(u, 0, lane, rows)
+        value = value + rz[0, 6 - u, rows, lane].astype(F32) + rz[1, 5 + u, rows, lane].astype(F32)
+        return (value * scale).T.astype(BF16)
+
+    gz[5][0].wait()
+    gz[6][0].wait()
+    for u in range(2):
+        fs_s[u, 0] = zlast(u, sides[0])
+        ops.send(fs_s.at[u, 0, cols(odd, RY), :], ow.at[u, :, there], Y2, small=True)
+        ops.send(fs_s.at[u, 0, cols(near, RY), :], ow.at[u, :, there], ACROSS, small=True)
+    gz[5][1].wait()
+    for part_of, rows in enumerate((TOP, LOW)):
+        gz[6][1 + part_of].wait()
+        lane = pl.ds(pl.multiple_of(y * HB + part_of * 128, 128), 128)
         for u in range(2):
-            value = total(u, 0, lane)
-            value = value + rz[0, 6 - u, :, lane].astype(F32) + rz[1, 5 + u, :, lane].astype(F32)
-            fs_s[u, half] = (value * scale).T.astype(BF16)
-            if half == 0:
-                odd = lax.rem(y, 2)
-                near = 1 - odd
-                ops.send(fs_s.at[u, 0, cols(odd, RY), :], ow.at[u, :, there], Y2, small=True)
-                ops.send(fs_s.at[u, 0, cols(near, RY), :], ow.at[u, :, there], ACROSS, small=True)
-            else:
-                odd = lax.rem(y, 2)
-                ops.send(fs_s.at[u, 1, cols(1 - odd, RY), :], ow.at[u, :, there], MATE, small=True)
-                ow[u, :, there] = fs_s[u, 1, cols(odd, RY), :]
+            fs_s[u, 1, :, rows] = zlast(u, sides[1], rows)
+            ops.send(fs_s.at[u, 1, cols(near, RY), rows], ow.at[u, :, lane], MATE, small=True)
+    for u in range(2):
+        ow[u, :, there] = fs_s[u, 1, cols(odd, RY), :]
 
     v1b.wait()
     finish_rows(0, q1[x] + rd[0].astype(F32) + rd[1].astype(F32), 0)

time: 88 us -> 85.9 us (0.976)
  Pallas kernels: 87.1 us -> 85 us
    pallas_call x1, Pallas kernels: 86.2 us -> 84.1 us  [per_device(): pl.pallas_call(kernel, out_shape=(bf(2, RY, 4 * HB), bf(2 * TB, 256)), in...]
where the time goes in v6:
time: 85.9 us; the launch traced here: 85.8 us
  Pallas kernels  85 us (99%)
    pallas_call x1, Pallas kernels, per_device(): pl.pallas_call(kernel, out_shape=(bf(2, RY, 4 * HB), bf(2 * TB, 256)), in...  84.1 us

profile of v6, /device:TPU:1, one launch (start us, length us, event | category | flops | bytes accessed | tf_op | source)
XLA Modules:
  0.0 85.8 jit_solution(11839664319176091148)
XLA Ops:
  0.6 84.1 %shard_map.67 = (bf16[2,64,1024]{2,1,0:T(8,128)(2,1)S(1)}, bf16[512,256]{1,0:T(8,128)(2,1)S(1)}) custom-call(bf16[512,256]{1,0:T(8,128)(2,1)} %x_in.1, bf16[512,256]{1,0:T(8,128)(2,1)} %c_in.1, bf16[64,1024]{1,0:T(8,128)(2,1)} %up_in.1, bf16[64,1024]{1,0:T(8,128)(2,1)} %bitcast.2), custom_call_target="tpu_custom_call" | custom-call | tf_op jit(solution)/shard_map/pallas_call | solution.py:527
  84.8 0.9 %shard_map.68 = (bf16[512,256]{1,0:T(8,128)(2,1)}, f32[64,1024]{1,0:T(8,128)}, f32[64,1024]{1,0:T(8,128)}) custom-call(bf16[2,64,1024]{2,1,0:T(8,128)(2,1)S(1)} %get-tuple-element.8.ow, bf16[512,256]{1,0:T(8,128)(2,1)S(1)} %get-tuple-element.9.og), custom_call_target="tpu_custom_call" | custom-call | tf_op jit(solution)/shard_map/pallas_call | solution.py:561

commit v7 on v6

--- a/solution.py
+++ b/solution.py
@@ -15,7 +15,7 @@
 DZ = 256
 RY = 64
 HALF = TB // 2
-CUT = 112
+CUT = 128
 MID = (96, 160)
 SENDS, RECVS = 6, 67
 MESH = pl.DeviceIdType.MESH
@@ -335,18 +335,21 @@
     early(*range(14))
 
     orow = slice(OPP * TB, OPP * TB + TB)
+    def gather_terms(n, buf, where, first=False):
+        for ax in where:
+            lane = cols(ax, FX)
+            more = nn(buf[orow, lane], w[n, lane, :])
+            acc[n] = more if first else acc[n] + more
+            first = False
+
     c3.wait()
+    gather_terms(1, cb, (x, xl, xr), True)
+    gather_terms(0, xb, (x,), True)
     fcx["2"].wait()
-    for h in range(2):
-        s = slice(h * HB, (h + 1) * HB)
-        acc[1, :, s] = nn(cb[orow], w[1, :, s])
-    early(14, 15)
+    gather_terms(1, cb, (x2,))
     fxy.wait()
     fmid.wait()
-    for n, ax in enumerate((x, xl, xr)):
-        lane = cols(ax, FX)
-        more = nn(xb[orow, lane], w[0, lane, :])
-        acc[0] = more if n == 0 else acc[0] + more
+    gather_terms(0, xb, (xl, xr))
     fxy2.wait()
     for h in (1, 0):
         s = slice(h * HB, (h + 1) * HB)
@@ -401,6 +404,7 @@
     for slot in (ME, L, R):
         last_x(slot)
     chunks(2)
+    early(14, 15)
     gsend(2)
     chunks(3)
     def next_y(n, r):

time: 85.9 us -> 85.8 us (level)
  no operation moved by 1% of the time
where the time goes in v7:
time: 85.8 us; the launch traced here: 85.7 us
  Pallas kernels  84.9 us (99%)
    pallas_call x1, Pallas kernels, per_device(): pl.pallas_call(kernel, out_shape=(bf(2, RY, 4 * HB), bf(2 * TB, 256)), in...  84 us

profile of v7, /device:TPU:1, one launch (start us, length us, event | category | flops | bytes accessed | tf_op | source)
XLA Modules:
  0.0 85.7 jit_solution(4748084550751424778)
XLA Ops:
  0.6 84.0 %shard_map.67 = (bf16[2,64,1024]{2,1,0:T(8,128)(2,1)S(1)}, bf16[512,256]{1,0:T(8,128)(2,1)S(1)}) custom-call(bf16[512,256]{1,0:T(8,128)(2,1)} %x_in.1, bf16[512,256]{1,0:T(8,128)(2,1)} %c_in.1, bf16[64,1024]{1,0:T(8,128)(2,1)} %up_in.1, bf16[64,1024]{1,0:T(8,128)(2,1)} %bitcast.2), custom_call_target="tpu_custom_call" | custom-call | tf_op jit(solution)/shard_map/pallas_call | solution.py:531
  84.6 0.9 %shard_map.68 = (bf16[512,256]{1,0:T(8,128)(2,1)}, f32[64,1024]{1,0:T(8,128)}, f32[64,1024]{1,0:T(8,128)}) custom-call(bf16[2,64,1024]{2,1,0:T(8,128)(2,1)S(1)} %get-tuple-element.8.ow, bf16[512,256]{1,0:T(8,128)(2,1)S(1)} %get-tuple-element.9.og), custom_call_target="tpu_custom_call" | custom-call | tf_op jit(solution)/shard_map/pallas_call | solution.py:565
